TPU v7x, 256 devices: a whole 4x4x8 slice. The times are simulated.
256 devices in a mesh: ep: 16 (over y, x), tp: 16 (over z, core).
Axes of the slice: x: 4, y: 4, z: 8, core: 2. Of those that a mesh axis runs over, the one named last changes fastest.
Arguments:
- mixer_input_rows: bfloat16 [32768, 2048], P(('ep', 'tp')), may hold values from -6 to 6
- mixer_norm_gain: float32 [2048], replicated, may hold values from 0.1 to 1.9
- query_weight: bfloat16 [2048, 2048], P(None, 'tp'), may hold values from -0.125 to 0.125
- key_weight: bfloat16 [2048, 2048], P(None, 'tp'), may hold values from -0.125 to 0.125
- value_weight: bfloat16 [2048, 2048], P(None, 'tp'), may hold values from -0.125 to 0.125
- write_strength_projection: bfloat16 [2048, 16], replicated, may hold values from -0.125 to 0.125
- decay_projection: bfloat16 [2048, 16], replicated, may hold values from -0.125 to 0.125
- head_decay_speed: float32 [16], P('tp'), may hold values from 0 to 1
- largest_write_strength: float32 [16], P('tp'), may hold values from 0 to 1
- extra_log_decay: float32 [32768, 16], P('ep', 'tp'), may hold values from -1 to 0
- head_norm_gain: float32 [128], replicated, may hold values from 0.1 to 1.9
- mixer_output_weight: bfloat16 [2048, 2048], P('tp'), may hold values from -0.125 to 0.125
- expert_input_rows: bfloat16 [2048, 2048], P(('ep', 'tp')), may hold values from -6 to 6
- expert_norm_gain: float32 [2048], replicated, may hold values from 0.1 to 1.9
- routes: int32 [2048, 2], P(('ep', 'tp')), may hold values from 0 to 15, all different within a row; in each aligned block of 8 rows (0 to 7, 8 to 15, ...) at most 2 rows name the same one
- expert_route_weight: float32 [2048, 2], P(('ep', 'tp')), may hold values from 0.2 to 1
- gate_weight: bfloat16 [16, 2048, 7168], P('ep', None, 'tp'), may hold values from -0.125 to 0.125
- up_weight: bfloat16 [16, 2048, 7168], P('ep', None, 'tp'), may hold values from -0.125 to 0.125
- down_weight: bfloat16 [16, 7168, 2048], P('ep', 'tp'), may hold values from -0.0625 to 0.0625
Outputs:
- mix_out: bfloat16 [32768, 2048], P(('ep', 'tp'))
- exp_out: bfloat16 [2048, 2048], P(('ep', 'tp'))
Inputs may be any that keep to these rules, and one draw needn't show every extreme that they name: `routes`: within the rows of one device (aligned blocks of 8 rows) no expert is named more than 2 times, some device names some expert exactly 2 times, and the 2 experts of a row differ.
All inputs are finite; a program needn't handle non-finite values.
Results may differ from a plain program's by a relative error of at most 0.019.
Values may be sent and summed in bfloat16 or wider, within the bound.
A program may use at most 128 MiB of HBM per device.

v0:
```python
import jax
import jax.numpy as jnp
from jax import lax
from jax.sharding import Mesh
from jax.sharding import PartitionSpec as P

HEAD = 128
BLOCK = 128
EP = ("ep_0", "ep_1")
TP = ("tp_0", "tp_1")
EP_TP = ("ep_0", "ep_1", "tp_0", "tp_1")


norm_eps = 1e-06
highest = lax.Precision.HIGHEST


def nothing_yet(x, identity):
    return jax.tree.map(
        lambda part, zero: jnp.zeros_like(part) + jnp.asarray(zero, part.dtype), x, identity
    )


def prefix_by_axis(x, axes, combine, identity):
    before = start = nothing_yet(x, identity)
    so_far = x
    for axis in reversed(axes):
        devices, here = (lax.axis_size(axis), lax.axis_index(axis))
        pieces = jax.tree.map(
            lambda part, kind: lax.all_gather(part.astype(kind), axis),
            so_far,
            jax.tree.map(lambda a: jnp.bfloat16 if a.dtype == jnp.float32 else a.dtype, x),
        )
        inside, so_far = (start, start)
        for k in range(devices):
            passed = k < here
            so_far = combine(
                so_far, jax.tree.map(lambda part, own: part[k].astype(own.dtype), pieces, x)
            )
            inside = jax.tree.map(lambda new, old: jnp.where(passed, new, old), so_far, inside)
        before = combine(inside, before)
    return before


def whole_of(x, axes, dim):
    for axis in reversed(axes):
        x = lax.all_gather(x, axis, axis=dim, tiled=True)
    return x


def cut_along(x, dim, devices):
    dims = x.shape
    parts = x.reshape(*dims[:dim], devices, dims[dim] // devices, *dims[dim + 1 :])
    return jnp.moveaxis(parts, dim, 0)


def sum_at_owner(x, axis, dim):
    devices = lax.axis_size(axis)
    parts = lax.all_to_all(cut_along(x, dim, devices), axis, 0, 0, tiled=True)
    return jnp.sum(parts.astype(jnp.float32), axis=0)


def rms_scale(rows_in, gain_vec):
    widened = rows_in.astype(jnp.float32)
    scaled = widened * lax.rsqrt(jnp.mean(widened * widened, axis=-1, keepdims=True) + norm_eps)
    return (scaled * gain_vec).astype(jnp.bfloat16)


def unit_rows(tensor):
    return tensor * lax.rsqrt(jnp.sum(tensor * tensor, axis=-1, keepdims=True) + 1e-06)


def block_terms(queries, key_rows, values, log_decay_values, strength):
    length = log_decay_values.shape[-1]
    cumulative = jnp.cumsum(log_decay_values, axis=-1)
    causal = jnp.tril(jnp.ones((length, length), jnp.bool_))
    strict = jnp.tril(jnp.ones((length, length), jnp.bool_), -1)
    decays = jnp.exp(
        jnp.where(causal, cumulative[..., :, None] - cumulative[..., None, :], -jnp.inf)
    )
    keys_scaled = key_rows * strength[..., None]
    inner_prod = jnp.einsum("...cd,...sd->...cs", keys_scaled, key_rows, precision=highest)
    system = jnp.where(strict, inner_prod * decays, 0.0) + jnp.eye(length, dtype=key_rows.dtype)
    right_side = jnp.concatenate(
        [values * strength[..., None], keys_scaled * jnp.exp(cumulative)[..., None]], axis=-1
    )
    solved = jax.scipy.linalg.solve_triangular(system, right_side, lower=True, unit_diagonal=True)
    value_width = values.shape[-1]
    carried = solved[..., :value_width]
    weights = solved[..., value_width:]
    scores = jnp.einsum("...cd,...sd->...cs", queries, key_rows, precision=highest) * decays
    query_dec = queries * jnp.exp(cumulative)[..., None]
    keys_dec = key_rows * jnp.exp(cumulative[..., -1:] - cumulative)[..., None]
    last_decay = jnp.exp(cumulative[..., -1])
    return (carried, weights, scores, query_dec, keys_dec, last_decay)


def apply_block(memory, carried, weights, scores, query_dec, keys_dec, last_decay):
    fresh_values = carried - jnp.einsum("...cd,...de->...ce", weights, memory, precision=highest)
    output = jnp.einsum("...cd,...de->...ce", query_dec, memory, precision=highest)
    output = output + jnp.einsum("...cs,...se->...ce", scores, fresh_values, precision=highest)
    memory = memory * last_decay[..., None, None] + jnp.einsum(
        "...cd,...ce->...de", keys_dec, fresh_values, precision=highest
    )
    return (memory, output)


def compose(earlier, later):
    first_map, first_shift = earlier
    second_map, second_shift = later
    joined_map = jnp.einsum("hij,hjk->hik", second_map, first_map, precision=highest)
    joined_shift = (
        jnp.einsum("hij,hjk->hik", second_map, first_shift, precision=highest) + second_shift
    )
    return (joined_map, joined_shift)


def delta_rule_kernel(
    projected_parts, head_decay_speed, largest_write_strength, extra_log_decay, head_norm_gain
):
    rows_total = projected_parts.shape[0]
    heads_here = head_decay_speed.shape[0]
    head_width = heads_here * HEAD
    queries = jax.nn.silu(projected_parts[:, :head_width]).reshape(rows_total, heads_here, HEAD)
    key_rows = unit_rows(
        jax.nn.silu(projected_parts[:, head_width : 2 * head_width]).reshape(
            rows_total, heads_here, HEAD
        )
    )
    values = jax.nn.silu(projected_parts[:, 2 * head_width : 3 * head_width]).reshape(
        rows_total, heads_here, HEAD
    )
    tail_start = 3 * head_width
    strength = largest_write_strength * jax.nn.sigmoid(
        projected_parts[:, tail_start : tail_start + heads_here]
    )
    log_decay_values = extra_log_decay - head_decay_speed * jax.nn.softplus(
        projected_parts[:, tail_start + heads_here : tail_start + 2 * heads_here]
    )
    block_count = rows_total // BLOCK

    def blocked(tensor):
        return tensor.reshape(block_count, BLOCK, heads_here, -1).transpose(0, 2, 1, 3)

    terms = block_terms(
        blocked(queries),
        blocked(key_rows),
        blocked(values),
        blocked(log_decay_values[..., None])[..., 0],
        blocked(strength[..., None])[..., 0],
    )
    carried, weights, scores, query_dec, keys_dec, last_decay = terms
    identity_map = jnp.eye(HEAD, dtype=jnp.float32)
    eye_maps = jnp.broadcast_to(identity_map, (heads_here, HEAD, HEAD))
    zero_shifts = jnp.zeros((heads_here, HEAD, HEAD), jnp.float32)
    block_maps = last_decay[..., None, None] * identity_map - jnp.einsum(
        "nhcd,nhce->nhde", keys_dec, weights, precision=highest
    )
    block_shifts = jnp.einsum("nhcd,nhce->nhde", keys_dec, carried, precision=highest)

    def compose_next(totals, pieces):
        return (compose(totals, pieces), None)

    span_pair, _ = lax.scan(compose_next, (eye_maps, zero_shifts), (block_maps, block_shifts))
    _, entering = prefix_by_axis(span_pair, EP, compose, (eye_maps, zero_shifts))

    def advance(memory, pieces):
        return apply_block(memory, *pieces)

    _, outputs = lax.scan(advance, entering, terms)
    heads_out = outputs.transpose(0, 2, 1, 3).reshape(rows_total, heads_here, HEAD)
    normalized = heads_out * lax.rsqrt(
        jnp.mean(heads_out * heads_out, axis=-1, keepdims=True) + norm_eps
    )
    normalized = normalized * head_norm_gain
    return normalized.reshape(rows_total, head_width).astype(jnp.bfloat16)


def expert_hidden(rows_in, gate_weight, up_weight):
    gate_part = jnp.dot(rows_in, gate_weight[0], preferred_element_type=jnp.float32)
    up_part = jnp.dot(rows_in, up_weight[0], preferred_element_type=jnp.float32)
    return (jax.nn.silu(gate_part) * up_part).astype(jnp.bfloat16)


def slot_numbers(routes, experts, capacity):
    assigned = routes.reshape(-1)
    onehot = (assigned[:, None] == jnp.arange(experts, dtype=jnp.int32)[None, :]).astype(jnp.int32)
    before = jnp.cumsum(onehot, axis=0) - onehot
    return assigned * capacity + jnp.sum(before * onehot, axis=1)


def body(
    mixer_input_rows,
    mixer_norm_gain,
    query_weight,
    key_weight,
    value_weight,
    write_strength_projection,
    decay_projection,
    head_decay_speed,
    largest_write_strength,
    extra_log_decay,
    head_norm_gain,
    mixer_output_weight,
    expert_input_rows,
    expert_norm_gain,
    routes,
    expert_route_weight,
    gate_weight,
    up_weight,
    down_weight,
):
    w_whole = lax.all_gather(mixer_output_weight, TP, axis=0, tiled=True)
    heads_here = head_decay_speed.shape[0]
    first_head = lax.axis_index(TP) * heads_here
    w_combined = jnp.concatenate(
        [
            query_weight,
            key_weight,
            value_weight,
            lax.dynamic_slice_in_dim(write_strength_projection, first_head, heads_here, 1),
            lax.dynamic_slice_in_dim(decay_projection, first_head, heads_here, 1),
        ],
        axis=1,
    )
    mix_normed = rms_scale(mixer_input_rows, mixer_norm_gain)
    exp_normed = rms_scale(expert_input_rows, expert_norm_gain)
    token_count, top_count = routes.shape
    model_width = exp_normed.shape[1]
    experts = gate_weight.shape[0] * lax.axis_size(EP)
    capacity = (3 * top_count * token_count + 2 * experts - 1) // (2 * experts)
    slot_ids = slot_numbers(routes, experts, capacity)
    places = jnp.arange(experts * capacity, dtype=jnp.int32)
    selector = jnp.sum(
        (slot_ids.reshape(token_count, top_count)[None, :, :] == places[:, None, None]).astype(
            jnp.float32
        ),
        axis=2,
    )
    sending = jnp.dot(
        selector.astype(jnp.bfloat16), exp_normed, preferred_element_type=jnp.float32
    ).astype(jnp.bfloat16)
    arrived = lax.all_to_all(
        sending.reshape(experts, capacity, model_width), EP, split_axis=0, concat_axis=0, tiled=True
    )
    arrived = arrived.reshape(-1, model_width)
    projected_parts = jnp.dot(
        lax.all_gather(mix_normed, TP, axis=0, tiled=True),
        w_combined,
        preferred_element_type=jnp.float32,
    )
    head_outputs_mixed = delta_rule_kernel(
        projected_parts, head_decay_speed, largest_write_strength, extra_log_decay, head_norm_gain
    )
    hidden = expert_hidden(whole_of(arrived, TP, 0), gate_weight, up_weight)
    local_heads = lax.all_to_all(head_outputs_mixed, TP, split_axis=0, concat_axis=1, tiled=True)
    groups = lax.axis_size(TP)
    group_width = head_outputs_mixed.shape[1]
    row_count = local_heads.shape[0]
    pieces = jnp.einsum(
        "rgk,gkd->grd",
        local_heads.reshape(row_count, groups, group_width),
        w_whole.reshape(groups, group_width, model_width),
        preferred_element_type=jnp.float32,
    ).astype(jnp.bfloat16)
    mix_sum = jnp.sum(lax.optimization_barrier(pieces).astype(jnp.float32), axis=0)
    expert_sum = sum_at_owner(
        jnp.dot(hidden, down_weight[0], preferred_element_type=jnp.float32).astype(jnp.bfloat16),
        TP,
        0,
    )
    finished = expert_sum.astype(jnp.bfloat16).reshape(experts, capacity, model_width)
    returned = lax.all_to_all(finished, EP, split_axis=0, concat_axis=0, tiled=True)
    results = returned.reshape(experts * capacity, model_width)[slot_ids].astype(jnp.float32)
    results = results.reshape(token_count, top_count, model_width)
    exp_out = jnp.sum(results * expert_route_weight[:, :, None], axis=1).astype(jnp.bfloat16)
    return (mix_sum.astype(jnp.bfloat16), exp_out)


def solution(mesh):
    torus = Mesh(mesh.devices.reshape(4, 4, 8, 2), ("ep_0", "ep_1", "tp_0", "tp_1"))
    placed = (
        P(EP_TP, None),
        P(),
        P(None, TP),
        P(None, TP),
        P(None, TP),
        P(),
        P(),
        P(TP),
        P(TP),
        P(EP, TP),
        P(),
        P(TP, None),
        P(EP_TP, None),
        P(),
        P(EP_TP, None),
        P(EP_TP, None),
        P(EP, None, TP),
        P(EP, None, TP),
        P(EP, TP, None),
    )
    return jax.shard_map(
        body,
        mesh=torus,
        in_specs=placed,
        out_specs=(P(EP_TP, None), P(EP_TP, None)),
        check_vma=False,
    )
```

profile of v0, /device:TPU:1, one launch (start us, length us, event | category | flops | bytes accessed | tf_op | source)
XLA Modules:
  0.0 563.3 jit_solution(5231713519708649916)
XLA Ops:
  10.8 14.2 %all_to_all.28 = bf16[16,2,2048]{2,1,0:T(2,128)(2,1)S(1)} all-to-all(bf16[16,2,2048]{2,1,0:T(2,128)(2,1)S(1)} %reshape.592), channel_id=1, replica_groups=mesh['ep_0'=4,'ep_1'=4,'tp_0'=8,'tp_1'=2] {'ep_0','ep_1'}, dimensions={0} | all-to-all | bytes 262144 | tf_op jit(solution)/shard_map/all_to_all | solution.py:243
  25.1 3.8 all_gather.46
  30.2 34.4 %all-gather.12.cloned.1.call-done = bf16[512,2048]{1,0:T(8,128)(2,1)} async-done(((bf16[64,2048]{1,0:T(8,128)(2,1)}), bf16[512,2048]{1,0:T(8,128)(2,1)}) %all-gather.12.cloned.1.call-update) | async-done | bytes 2097168 | tf_op jit(solution)/shard_map/all_gather | solution.py:47
  68.0 5.9 %convolution_convert_fusion.1 = bf16[512,2048]{1,0:T(8,128)(2,1)} fusion(bf16[1,448,2048]{2,1,0:T(8,128)(2,1)S(1)} %copy-done, bf16[512,2048]{1,0:T(8,128)(2,1)} %all-gather.12.cloned.1.call-done, bf16[1,2048,448]{1,2,0:T(8,128)(2,1)} %param.40, f32[512,448]{0,1:T(8,128)S(1)} %fusion.33), kind=kOutput, calls=%fused_computation.35 | convolution fusion | flops 1881473024 | bytes 8781824 | tf_op jit(solution)/shard_map/dot_general | solution.py:268
  73.9 9.3 %all-to-all-start.2 = ((bf16[16,32,2048]{2,1,0:T(8,128)(2,1)}), bf16[16,32,2048]{2,1,0:T(8,128)(2,1)}, u32[]{:S(2)}, u32[]{:S(2)}) async-start(bf16[16,32,2048]{2,1,0:T(8,128)(2,1)} %bitcast.254), calls=%async_computation.2 | async-start | bytes 4194304 | tf_op jit(solution)/shard_map/all_to_all | solution.py:59
  86.7 4.0 concatenate.6
  90.8 63.1 %all-to-all-done.2 = bf16[16,32,2048]{2,1,0:T(8,128)(2,1)} async-done(((bf16[16,32,2048]{2,1,0:T(8,128)(2,1)}), bf16[16,32,2048]{2,1,0:T(8,128)(2,1)}, u32[]{:S(2)}, u32[]{:S(2)}) %all-to-all-start.2) | async-done | bytes 2097184 | tf_op jit(solution)/shard_map/all_to_all | solution.py:59
  156.6 6.5 %all-to-all-start.3 = ((bf16[16,2,2048]{2,1,0:T(2,128)(2,1)}), bf16[16,2,2048]{2,1,0:T(2,128)(2,1)S(1)}, u32[]{:S(2)}, u32[]{:S(2)}) async-start(bf16[16,2,2048]{2,1,0:T(2,128)(2,1)} %reshape.595), calls=%async_computation.3 | async-start | bytes 262144 | tf_op jit(solution)/shard_map/all_to_all | solution.py:273
  163.2 7.8 %all-gather.8.cloned.1.call-done = bf16[2048,2048]{1,0:T(8,128)(2,1)} async-done(((bf16[128,2048]{1,0:T(8,128)(2,1)}), bf16[2048,2048]{1,0:T(8,128)(2,1)}) %all-gather.8.cloned.1.call-update) | async-done | bytes 8388624 | tf_op jit(solution)/shard_map/all_gather | solution.py:248
  171.1 6.6 %fusion.140 = f32[2048,386]{0,1:T(8,128)S(1)} fusion(bf16[2048,2048]{1,0:T(8,128)(2,1)} %all-gather.8.cloned.1.call-done, bf16[2048,386]{1,0:T(8,128)(2,1)} %concatenate.6), kind=kOutput, calls=%fused_computation.198 | convolution fusion | flops 3238002688 | bytes 13131776 | tf_op jit(solution)/shard_map/dot_general | solution.py:247
  180.1 4.0 multiply_bitcast_fusion.1
  190.1 4.7 fusion.41
  194.8 3.3 fusion.55
  198.2 158.6 %custom-call.4 = f32[16,1,128,128]{2,3,1,0:T(8,128)} custom-call(f32[16,1,128,128]{3,2,1,0:T(8,128)} %fusion.55), custom_call_target="InvertDiagBlocksLowerTriangular" | custom-call | tf_op jit(solution)/shard_map/jit(_solve_triangular)/vmap()/triangular_solve | solution.py:87
  369.2 21.0 %while.24 = (s32[]{:T(128)}, f32[1,128,128]{2,1,0:T(8,128)S(1)}, f32[1,128,128]{2,1,0:T(8,128)S(1)}, f32[16,1,128,128]{3,2,1,0:T(8,128)S(1)}, f32[16,1,128,128]{3,2,1,0:T(8,128)}, /*index=5*/s32[]{:T(128)}) while((s32[]{:T(128)}, f32[1,128,128]{2,1,0:T(8,128)S(1)}, f32[1,128,128]{2,1,0:T(8,128)S(1)}, f32[16,1,128,128]{3,2,1,0:T(8,128)S(1)}, ...), condition=%wide.region_4.5_spmd, body=%wide.region_3.4_spmd.sunk | while | flops 50348032 | bytes 721993 | solution.py:164
  390.2 10.0 %all-gather = bf16[4,128,128]{2,1,0:T(8,128)(2,1)S(1)} all-gather(bf16[1,128,128]{2,1,0:T(8,128)(2,1)S(1)} %convert_element_type.154), channel_id=2, replica_groups=mesh['ep_0'=4,'ep_1'=4,'tp_0'=8,'tp_1'=2] {'ep_1'}, dimensions={0}, use_global_device_ids=true | all-gather | bytes 163840 | tf_op jit(solution)/shard_map/all_gather | solution.py:30
  400.2 9.1 %all-gather.2 = bf16[4,128,128]{2,1,0:T(8,128)(2,1)S(1)} all-gather(bf16[1,128,128]{2,1,0:T(8,128)(2,1)S(1)} %convert_element_type.156), channel_id=4, replica_groups=mesh['ep_0'=4,'ep_1'=4,'tp_0'=8,'tp_1'=2] {'ep_1'}, dimensions={0}, use_global_device_ids=true | all-gather | bytes 163840 | tf_op jit(solution)/shard_map/all_gather | solution.py:30
  410.2 9.4 %all-gather.3 = bf16[512,128]{1,0:T(8,128)(2,1)S(1)} all-gather(bf16[128,128]{1,0:T(8,128)(2,1)S(1)} %get-tuple-element.181), channel_id=5, replica_groups=mesh['ep_0'=4,'ep_1'=4,'tp_0'=8,'tp_1'=2] {'ep_0'}, dimensions={0}, use_global_device_ids=true | all-gather | bytes 163840 | tf_op jit(solution)/shard_map/all_gather | solution.py:30
  420.2 9.2 %all-gather.1 = bf16[512,128]{1,0:T(8,128)(2,1)S(1)} all-gather(bf16[128,128]{1,0:T(8,128)(2,1)S(1)} %get-tuple-element.183), channel_id=3, replica_groups=mesh['ep_0'=4,'ep_1'=4,'tp_0'=8,'tp_1'=2] {'ep_0'}, dimensions={0}, use_global_device_ids=true | all-gather | bytes 163840 | tf_op jit(solution)/shard_map/all_gather | solution.py:30
  431.2 76.0 %while.25 = (s32[]{:T(128)}, f32[1,128,128]{2,1,0:T(8,128)S(1)}, f32[16,1,128,128]{3,2,1,0:T(8,128)S(1)}, f32[16,1]{0,1:T(1,128)S(1)}, f32[16,1,128,128]{3,2,1,0...) while((s32[]{:T(128)}, f32[1,128,128]{2,1,0:T(8,128)S(1)}, ...), condition=%wide.region_6.7_spmd, body=%wide.region_5.6_spmd.sunk | while | flops 100728832 | bytes 985721 | solution.py:170
  508.7 15.7 %all-to-all-start = ((bf16[16,128,128]{2,1,0:T(8,128)(2,1)}), bf16[16,128,128]{2,1,0:T(8,128)(2,1)S(1)}, u32[]{:S(2)}, u32[]{:S(2)}) async-start(bf16[16,128,128]{2,1,0:T(8,128)(2,1)} %fusion.70), calls=%async_computation | async-start | bytes 1048576 | tf_op jit(solution)/shard_map/all_to_all | solution.py:256
  526.2 15.4 %all-to-all-done = bf16[16,128,128]{2,1,0:T(8,128)(2,1)S(1)} async-done(((bf16[16,128,128]{2,1,0:T(8,128)(2,1)}), bf16[16,128,128]{2,1,0:T(8,128)(2,1)S(1)}, u32[]{:S(2)}, u32[]{:S(2)}) %all-to-all-start) | async-done | bytes 524320 | tf_op jit(solution)/shard_map/all_to_all | solution.py:256
  541.6 8.9 %convolution_convert_fusion = bf16[16,128,2048]{2,1,0:T(8,128)(2,1)} fusion(bf16[16,128,2048]{2,1,0:T(8,128)(2,1)} %bitcast.247, bf16[16,128,128]{2,1,0:T(8,128)(2,1)S(1)} %all-to-all-done), kind=kOutput, calls=%fused_computation.34 | convolution fusion | flops 1077936128 | bytes 17301504 | tf_op jit(solution)/shard_map/rgk,gkd->grd/dot_general | solution.py:260
  550.5 6.3 %reduce_sum.94 = bf16[128,2048]{1,0:T(8,128)(2,1)} reduce(bf16[16,128,2048]{2,1,0:T(8,128)(2,1)} %convolution_convert_fusion, bf16[]{:T(256)} %constant.104.clone.1), dimensions={0}, to_apply=%region_8.9 | reduce | flops 3932160 | bytes 8912898 | tf_op jit(solution)/shard_map/reduce_sum | solution.py:266
  (258 shorter events, 135.8 us)
Async XLA Ops:
  7.2 60.8 %copy-start = (bf16[1,448,2048]{2,1,0:T(8,128)(2,1)S(1)}, bf16[1,448,2048]{2,1,0:T(8,128)(2,1)}, u32[]{:S(2)}) copy-start(bf16[1,448,2048]{2,1,0:T(8,128)(2,1)} %param.41) | copy-start | bytes 5505028
  7.2 21.8 %copy-start.6 = (bf16[128,2048]{1,0:T(8,128)(2,1)S(1)}, bf16[128,2048]{1,0:T(8,128)(2,1)}, u32[]{:S(2)}) copy-start(bf16[128,2048]{1,0:T(8,128)(2,1)} %param.23) | copy-start | bytes 1572868
  7.2 22.0 %copy-start.11 = (f32[2048]{0:T(1024)S(1)}, f32[2048]{0:T(1024)}, u32[]{:S(2)}) copy-start(f32[2048]{0:T(1024)} %param.24) | copy-start | bytes 24580
  7.2 57.5 %all-gather.12.cloned.1.call-start = ((), (), s32[]{:S(2)}) async-start(), calls=%async_computation.6 | async-start | bytes 2359296 | tf_op jit(solution)/shard_map/all_gather | solution.py:47
  29.0 142.1 %all-gather.8.cloned.1.call-start = ((), (), s32[]{:S(2)}) async-start(), calls=%async_computation.4 | async-start | bytes 8912896 | tf_op jit(solution)/shard_map/all_gather | solution.py:248
  73.8 12.8 %copy-start.8 = (bf16[2048,128]{1,0:T(8,128)(2,1)S(1)}, bf16[2048,128]{1,0:T(8,128)(2,1)}, u32[]{:S(2)}) copy-start(bf16[2048,128]{1,0:T(8,128)(2,1)} %param.25) | copy-start | bytes 1572868
  73.8 12.8 %copy-start.9 = (bf16[2048,128]{1,0:T(8,128)(2,1)S(1)}, bf16[2048,128]{1,0:T(8,128)(2,1)}, u32[]{:S(2)}) copy-start(bf16[2048,128]{1,0:T(8,128)(2,1)} %param.26) | copy-start | bytes 1572868
  73.8 12.8 %copy-start.10 = (bf16[2048,128]{1,0:T(8,128)(2,1)S(1)}, bf16[2048,128]{1,0:T(8,128)(2,1)}, u32[]{:S(2)}) copy-start(bf16[2048,128]{1,0:T(8,128)(2,1)} %param.27) | copy-start | bytes 1572868
  73.9 80.0 %all-to-all-start.2 = ((bf16[16,32,2048]{2,1,0:T(8,128)(2,1)}), bf16[16,32,2048]{2,1,0:T(8,128)(2,1)}, u32[]{:S(2)}, u32[]{:S(2)}) async-start(bf16[16,32,2048]{2,1,0:T(8,128)(2,1)} %bitcast.254), calls=%async_computation.2 | async-start | bytes 4194304 | tf_op jit(solution)/shard_map/all_to_all | solution.py:59
  83.1 443.0 %all-gather.10.cloned.1.call-start = ((), (), s32[]{:S(2)}) async-start(), calls=%async_computation.5 | async-start | bytes 8912896 | tf_op jit(solution)/shard_map/all_gather | solution.py:213
  156.6 352.1 %all-to-all-start.3 = ((bf16[16,2,2048]{2,1,0:T(2,128)(2,1)}), bf16[16,2,2048]{2,1,0:T(2,128)(2,1)S(1)}, u32[]{:S(2)}, u32[]{:S(2)}) async-start(bf16[16,2,2048]{2,1,0:T(2,128)(2,1)} %reshape.595), calls=%async_computation.3 | async-start | bytes 262144 | tf_op jit(solution)/shard_map/all_to_all | solution.py:273
  163.2 16.2 %copy-start.12 = (f32[2048,1]{0,1:T(1,128)S(1)}, f32[2048,1]{0,1:T(1,128)}, u32[]{:S(2)}) copy-start(f32[2048,1]{0,1:T(1,128)} %param.32) | copy-start | bytes 24580
  177.7 1.7 copy-start.2
  190.1 4.7 copy-start.3
  359.3 2.8 copy-start.7
  390.2 39.8 %copy-start.5 = (f32[16,1,128,128]{3,2,1,0:T(8,128)S(1)}, f32[16,1,128,128]{3,2,1,0:T(8,128)}, u32[]{:S(2)}) copy-start(f32[16,1,128,128]{3,2,1,0:T(8,128)} %copy.94) | copy-start | bytes 3145732
  420.0 11.1 %copy-start.4 = (f32[16,1,128,128]{3,2,1,0:T(8,128)S(1)}, f32[16,1,128,128]{3,2,1,0:T(8,128)}, u32[]{:S(2)}) copy-start(f32[16,1,128,128]{3,2,1,0:T(8,128)} %custom-call.7) | copy-start | bytes 3145732
  431.2 76.4 %copy-start.14 = (f32[128]{0:T(128)S(1)}, f32[128]{0:T(128)}, u32[]{:S(2)}) copy-start(f32[128]{0:T(128)} %param.33) | copy-start | bytes 1540
  507.2 17.3 %copy-start.13 = (f32[8,2]{0,1:T(2,128)S(1)}, f32[8,2]{0,1:T(2,128)}, u32[]{:S(2)}) copy-start(f32[8,2]{0,1:T(2,128)} %param.38) | copy-start | bytes 196
  508.7 32.9 %all-to-all-start = ((bf16[16,128,128]{2,1,0:T(8,128)(2,1)}), bf16[16,128,128]{2,1,0:T(8,128)(2,1)S(1)}, u32[]{:S(2)}, u32[]{:S(2)}) async-start(bf16[16,128,128]{2,1,0:T(8,128)(2,1)} %fusion.70), calls=%async_computation | async-start | bytes 1048576 | tf_op jit(solution)/shard_map/all_to_all | solution.py:256
  550.5 6.3 %copy-start.1 = (bf16[1,448,2048]{2,1,0:T(8,128)(2,1)S(1)}, bf16[1,448,2048]{2,1,0:T(8,128)(2,1)}, u32[]{:S(2)}) copy-start(bf16[1,448,2048]{2,1,0:T(8,128)(2,1)} %param.41) | copy-start | bytes 5505028
Sparse Core Ops, SparseCore 0:
  29.1 35.5 all-gather.11
  67.1 103.9 all-gather.7
  172.9 54.4 all-gather.9
where the time goes:
time: 567 us; the launch traced here: 563 us
  other arithmetic  180 us (32%)
  matrix products  128 us (23%)
  waiting for transfers between devices  121 us (21%)
  blocking collectives  55.8 us (10%)
  starting transfers between devices  31.6 us (6%)
  local copies, waits for them, and re-layouts  29.8 us (5%)
  between operations  15.5 us (3%)
    another operation x3, other arithmetic, block_terms(): jax.scipy.linalg.solve_triangular(system, right_side, lower=True, unit_di...  159 us
    all_to_all x1, waiting for transfers between devices, sum_at_owner(): parts = lax.all_to_all(cut_along(x, dim, devices), axis, 0, 0, tiled=True)  63.1 us
    all_gather x4, blocking collectives, prefix_by_axis(): lax.all_gather(part.astype(kind), axis)  37.8 us
    all_gather x1, waiting for transfers between devices, whole_of(): x = lax.all_gather(x, axis, axis=dim, tiled=True)  34.4 us
    dot_general x26, matrix products, compose(): jnp.einsum('hij,hjk->hik', second_map, first_shift, precision=highest)  18.6 us
    dot_general x16, matrix products, apply_block(): jnp.einsum('...cd,...de->...ce', weights, memory, precision=highest)  17.3 us
    dot_general x16, matrix products, apply_block(): jnp.einsum('...cs,...se->...ce', scores, fresh_values, precision=highest)  16.8 us
    dot_general x16, matrix products, apply_block(): jnp.einsum('...cd,...de->...ce', query_dec, memory, precision=highest)  16.7 us
  transfers between devices with their start and end apart: 6, of which 4 were waited for; matrix products, arithmetic and copies ran while one was open for 56% of the time, Pallas kernels for 0%

commit v1 on v0

v1 whole, which is shorter than its diff:
```python
import functools

import jax
import jax.numpy as jnp
from jax import lax
from jax.experimental import pallas as pl
from jax.experimental.pallas import tpu as pltpu
from jax.sharding import Mesh
from jax.sharding import PartitionSpec as P

HEAD = 128
BLOCK = 128
EP = ("ep_0", "ep_1")
TP = ("tp_0", "tp_1")
EP_TP = ("ep_0", "ep_1", "tp_0", "tp_1")
MESH = pl.DeviceIdType.MESH

norm_eps = 1e-06
f32 = jnp.float32
bf16 = jnp.bfloat16


def mm(a, b):
    return jnp.dot(a.astype(bf16), b.astype(bf16), preferred_element_type=f32)


def mm_nt(a, b):
    return lax.dot_general(
        a.astype(bf16), b.astype(bf16), (((1,), (1,)), ((), ())), preferred_element_type=f32
    )


def whole_of(x, axes, dim):
    for axis in reversed(axes):
        x = lax.all_gather(x, axis, axis=dim, tiled=True)
    return x


def cut_along(x, dim, devices):
    dims = x.shape
    parts = x.reshape(*dims[:dim], devices, dims[dim] // devices, *dims[dim + 1 :])
    return jnp.moveaxis(parts, dim, 0)


def sum_at_owner(x, axis, dim):
    devices = lax.axis_size(axis)
    parts = lax.all_to_all(cut_along(x, dim, devices), axis, 0, 0, tiled=True)
    return jnp.sum(parts.astype(f32), axis=0)


def rms_scale(rows_in, gain_vec):
    widened = rows_in.astype(f32)
    scaled = widened * lax.rsqrt(jnp.mean(widened * widened, axis=-1, keepdims=True) + norm_eps)
    return (scaled * gain_vec).astype(bf16)


def silu(v):
    return v / (1.0 + jnp.exp(-v))


def invert(system):
    row = lax.broadcasted_iota(jnp.int32, (BLOCK, BLOCK), 0)
    col = lax.broadcasted_iota(jnp.int32, (BLOCK, BLOCK), 1)
    apart = row ^ col
    inverse = jnp.where(row == col, 1.0, 0.0) - jnp.where(apart == 1, system, 0.0)
    size = 2
    while size < BLOCK:
        corner = jnp.where((apart >= size) & (apart < 2 * size), system, 0.0)
        rounded = inverse.astype(bf16)
        inverse = inverse - mm(mm(rounded, corner), rounded)
        size *= 2
    return inverse


def block_maps(q, k, v, strength, log_decay):
    row = lax.broadcasted_iota(jnp.int32, (BLOCK, BLOCK), 0)
    col = lax.broadcasted_iota(jnp.int32, (BLOCK, BLOCK), 1)
    lower = jnp.where(row >= col, 1.0, 0.0).astype(bf16)
    high = log_decay.astype(bf16)
    rest = log_decay - high.astype(f32)
    middle = rest.astype(bf16)
    low = (rest - middle.astype(f32)).astype(bf16)
    total = mm(lower, high) + mm(lower, middle) + mm(lower, low)
    decays = jnp.exp(jnp.where(row >= col, total - total.T, -1e30))
    both = mm_nt(jnp.concatenate([q, k], axis=0), k)
    scores = both[:BLOCK] * decays
    system = jnp.where(row > col, both[BLOCK:] * strength * decays, 0.0)
    inverse = invert(system)
    grown = jnp.exp(total)
    right = jnp.concatenate([strength * grown * k, strength * v], axis=1)
    solved = mm(inverse, right)
    last = total[BLOCK - 1 : BLOCK, :]
    keys_left = k * jnp.exp(last - total)
    joined = mm(jnp.concatenate([scores, keys_left.T], axis=0), solved)
    return (
        q * grown - joined[:BLOCK, :HEAD],
        joined[:BLOCK, HEAD:],
        joined[BLOCK:, :HEAD],
        joined[BLOCK:, HEAD:],
        jnp.exp(last),
    )


def project_pair(x, w_all, extra, speed, largest):
    p = jnp.dot(x, w_all, preferred_element_type=f32)
    q = silu(p[:, :HEAD])
    k = silu(p[:, HEAD : 2 * HEAD])
    k = k * lax.rsqrt(jnp.sum(k * k, axis=-1, keepdims=True) + 1e-06)
    v = silu(p[:, 2 * HEAD : 3 * HEAD])
    strength = largest / (1.0 + jnp.exp(-p[:, 3 * HEAD : 4 * HEAD]))
    raw = p[:, 4 * HEAD : 5 * HEAD]
    softplus = jnp.maximum(raw, 0.0) + jnp.log(1.0 + jnp.exp(-jnp.abs(raw)))
    return q, k, v, strength, extra - speed * softplus


def pair_maps(x, w_all, extra, speed, largest):
    q, k, v, strength, log_decay = project_pair(x, w_all, extra, speed, largest)
    cut = lambda a, i: a[i * BLOCK : (i + 1) * BLOCK]
    qa, oa, ga, sa, da = block_maps(*[cut(a, 0) for a in (q, k, v, strength, log_decay)])
    qb, ob, gb, sb, db = block_maps(*[cut(a, 1) for a in (q, k, v, strength, log_decay)])
    t = mm(jnp.concatenate([gb, qb], axis=0), jnp.concatenate([ga, sa], axis=1))
    g = db * ga + da * gb - t[:BLOCK, :HEAD]
    s = db * sa - t[:BLOCK, HEAD:] + sb
    qb = da * qb - t[BLOCK:, :HEAD]
    ob = t[BLOCK:, HEAD:] + ob
    return jnp.concatenate([qa, qb], axis=0), jnp.concatenate([oa, ob], axis=0), g, s, da * db


def fill_weights(w_all, wq_ref, wk_ref, wv_ref, ws_ref, wd_ref, head):
    w_all[:, 0:HEAD] = wq_ref[...]
    w_all[:, HEAD : 2 * HEAD] = wk_ref[...]
    w_all[:, 2 * HEAD : 3 * HEAD] = wv_ref[...]
    heads = ws_ref.shape[1]
    pick = jnp.where(lax.broadcasted_iota(jnp.int32, (heads, HEAD), 0) == head, 1.0, 0.0)
    w_all[:, 3 * HEAD : 4 * HEAD] = mm(ws_ref[...], pick).astype(bf16)
    w_all[:, 4 * HEAD : 5 * HEAD] = mm(wd_ref[...], pick).astype(bf16)


def span_chain(pairs, lhs_s, g_s, s_s, o_s, d_s, ps_ref, qh_ref, oh_ref):
    g = jnp.zeros((HEAD, HEAD), f32)
    s = jnp.zeros((HEAD, HEAD), f32)
    d = jnp.ones((1, HEAD), f32)
    for z in range(pairs):
        rows = pl.ds(z * 2 * BLOCK, 2 * BLOCK)
        lhs = lhs_s[z]
        t = mm(lhs, jnp.concatenate([g, s], axis=1))
        qh_ref[rows, :] = (d * lhs[HEAD:].astype(f32) - t[HEAD:, :HEAD]).astype(bf16)
        oh_ref[rows, :] = t[HEAD:, HEAD:] + o_s[z]
        dz = d_s[z, 0:1, :]
        g, s = dz * g + d * g_s[z] - t[:HEAD, :HEAD], dz * s - t[:HEAD, HEAD:] + s_s[z]
        d = d * dz
    row = lax.broadcasted_iota(jnp.int32, (HEAD, HEAD), 0)
    col = lax.broadcasted_iota(jnp.int32, (HEAD, HEAD), 1)
    ps_ref[:, :HEAD] = (jnp.where(row == col, d, 0.0) - g).astype(bf16)
    ps_ref[:, HEAD:] = s.astype(bf16)


def span_kernel(
    x_ref, wq_ref, wk_ref, wv_ref, ws_ref, wd_ref, speed_ref, largest_ref, extra_ref,
    ps_ref, qh_ref, oh_ref,
    w_all, lhs_s, g_s, s_s, o_s, d_s,
):
    head = lax.axis_index("tp_0") * 2 + lax.axis_index("tp_1")
    pairs = x_ref.shape[0] // (2 * BLOCK)
    fill_weights(w_all, wq_ref, wk_ref, wv_ref, ws_ref, wd_ref, head)

    def step(z, carry):
        rows = pl.ds(pl.multiple_of(z * 2 * BLOCK, 2 * BLOCK), 2 * BLOCK)
        q, o, g, s, d = pair_maps(
            x_ref[rows, :], w_all[...], extra_ref[rows, :], speed_ref[0], largest_ref[0]
        )
        lhs_s[z, :HEAD] = g.astype(bf16)
        lhs_s[z, HEAD:] = q.astype(bf16)
        o_s[z] = o
        g_s[z] = g
        s_s[z] = s
        d_s[z] = jnp.broadcast_to(d, (8, HEAD))
        return carry

    lax.fori_loop(0, pairs, step, 0)
    span_chain(pairs, lhs_s, g_s, s_s, o_s, d_s, ps_ref, qh_ref, oh_ref)


def span_scratch(model, pairs):
    return [
        pltpu.VMEM((model, 5 * HEAD), bf16),
        pltpu.VMEM((pairs, 3 * HEAD, HEAD), bf16),
        pltpu.VMEM((pairs, HEAD, HEAD), f32),
        pltpu.VMEM((pairs, HEAD, HEAD), f32),
        pltpu.VMEM((pairs, 2 * BLOCK, HEAD), f32),
        pltpu.VMEM((pairs, 8, HEAD), f32),
    ]


def span_call(x_rows, wq, wk, wv, ws, wd, speed, largest, extra):
    rows, model = x_rows.shape
    pairs = rows // (2 * BLOCK)
    vm = pl.BlockSpec(memory_space=pltpu.VMEM)
    sm = pl.BlockSpec(memory_space=pltpu.SMEM)
    return pl.pallas_call(
        span_kernel,
        out_shape=(
            jax.ShapeDtypeStruct((HEAD, 2 * HEAD), bf16),
            jax.ShapeDtypeStruct((rows, HEAD), bf16),
            jax.ShapeDtypeStruct((rows, HEAD), f32),
        ),
        in_specs=[vm, vm, vm, vm, vm, vm, sm, sm, vm],
        out_specs=(vm, vm, vm),
        scratch_shapes=span_scratch(model, pairs),
        compiler_params=pltpu.CompilerParams(vmem_limit_bytes=56 * 1024 * 1024),
        cost_estimate=pl.CostEstimate(
            flops=30_000_000_000, bytes_accessed=16 * 1024 * 1024, transcendentals=0
        ),
        name="span",
    )(x_rows, wq, wk, wv, ws, wd, speed, largest, extra)


def mix_kernel(
    ps_ref, qh_ref, oh_ref, gain_ref, w_ref, out_ref,
    row_maps, col_maps, total_s, heads_out, heads_in, w_s,
    w_sem, send_sem, row_sem, col_sem, head_send, head_sem,
):
    y, x = lax.axis_index("ep_0"), lax.axis_index("ep_1")
    z, c = lax.axis_index("tp_0"), lax.axis_index("tp_1")
    t = z * 2 + c
    groups = heads_in.shape[1] // HEAD
    w_copy = pltpu.make_async_copy(w_ref, w_s, w_sem)
    w_copy.start()

    barrier = pltpu.get_barrier_semaphore()
    for j in range(1, 4):
        pl.semaphore_signal(barrier, 1, device_id={"ep_1": (x + j) % 4}, device_id_type=MESH)
        pl.semaphore_signal(barrier, 1, device_id={"ep_0": (y + j) % 4}, device_id_type=MESH)
    for j in range(1, 16):
        o = (t + j) % 16
        pl.semaphore_signal(
            barrier, 1, device_id={"tp_0": o // 2, "tp_1": o % 2}, device_id_type=MESH
        )
    pl.semaphore_wait(barrier, 21)

    sends = []
    for j in range(1, 4):
        sends.append(
            pltpu.make_async_remote_copy(
                ps_ref, row_maps.at[x], send_sem.at[j], row_sem.at[x],
                device_id={"ep_1": (x + j) % 4}, device_id_type=MESH,
            )
        )
    for copy in sends:
        copy.start()
    row_maps[x] = ps_ref[...]
    for j in range(1, 4):
        o = (x + j) % 4
        pltpu.make_async_remote_copy(
            ps_ref, row_maps.at[o], send_sem.at[0], row_sem.at[o],
            device_id={"ep_1": o}, device_id_type=MESH,
        ).wait_recv()

    whole = row_maps[0]
    before = whole
    for k in range(1, 4):
        before = jnp.where(x == k, whole, before)
        later = row_maps[k]
        step = mm(later[:, :HEAD], whole)
        whole = jnp.concatenate(
            [step[:, :HEAD], step[:, HEAD:] + later[:, HEAD:].astype(f32)], axis=1
        ).astype(bf16)
    total_s[...] = whole
    sends2 = []
    for j in range(1, 4):
        sends2.append(
            pltpu.make_async_remote_copy(
                total_s, col_maps.at[y], send_sem.at[3 + j], col_sem.at[y],
                device_id={"ep_0": (y + j) % 4}, device_id_type=MESH,
            )
        )
    for copy in sends2:
        copy.start()
    col_maps[y] = whole
    for j in range(1, 4):
        o = (y + j) % 4
        pltpu.make_async_remote_copy(
            total_s, col_maps.at[o], send_sem.at[0], col_sem.at[o],
            device_id={"ep_0": o}, device_id_type=MESH,
        ).wait_recv()
    memory = jnp.zeros((HEAD, HEAD), f32)
    for k in range(3):
        earlier = col_maps[k]
        moved = earlier[:, HEAD:].astype(f32)
        if k:
            moved = moved + mm(earlier[:, :HEAD], memory)
        memory = jnp.where(k < y, moved, memory)
    moved = mm(before[:, :HEAD], memory) + before[:, HEAD:].astype(f32)
    memory = jnp.where(x > 0, moved, memory).astype(bf16)

    gain = gain_ref[...]

    def finish(n, carry):
        rows = pl.ds(pl.multiple_of(n * 2 * BLOCK, 2 * BLOCK), 2 * BLOCK)
        o = mm(qh_ref[rows, :], memory) + oh_ref[rows, :]
        o = o * lax.rsqrt(jnp.mean(o * o, axis=-1, keepdims=True) + norm_eps)
        heads_out[rows, :] = (o * gain).astype(bf16)
        return carry

    lax.fori_loop(0, groups // 2, finish, 0, unroll=True)
    mine = pl.ds(pl.multiple_of(t * HEAD, HEAD), HEAD)
    head_copies = []
    for j in range(1, 16):
        o = (t + j) % 16
        rows = pl.ds(pl.multiple_of(o * BLOCK, BLOCK), BLOCK)
        copy = pltpu.make_async_remote_copy(
            heads_out.at[rows, :], heads_in.at[:, mine], head_send.at[j], head_sem.at[t],
            device_id={"tp_0": o // 2, "tp_1": o % 2}, device_id_type=MESH,
        )
        head_copies.append(copy)
        copy.start()
    heads_in[:, mine] = heads_out[pl.ds(pl.multiple_of(t * BLOCK, BLOCK), BLOCK), :]
    for j in range(1, 16):
        o = (t + j) % 16
        cols = pl.ds(pl.multiple_of(o * HEAD, HEAD), HEAD)
        pltpu.make_async_remote_copy(
            heads_out.at[pl.ds(0, BLOCK), :], heads_in.at[:, cols], head_send.at[0], head_sem.at[o],
            device_id={"tp_0": o // 2, "tp_1": o % 2}, device_id_type=MESH,
        ).wait_recv()
    w_copy.wait()
    tile = 512

    def project(n, carry):
        cols = pl.ds(pl.multiple_of(n * tile, tile), tile)
        out_ref[:, cols] = jnp.dot(
            heads_in[...], w_s[:, cols], preferred_element_type=f32
        ).astype(bf16)
        return carry

    lax.fori_loop(0, out_ref.shape[1] // tile, project, 0)
    for copy in sends + sends2 + head_copies:
        copy.wait_send()


def mix_call(ps, qh, oh, gain, w_whole):
    rows = qh.shape[0]
    model = w_whole.shape[1]
    vm = pl.BlockSpec(memory_space=pltpu.VMEM)
    return pl.pallas_call(
        mix_kernel,
        out_shape=jax.ShapeDtypeStruct((BLOCK, model), bf16),
        in_specs=[vm, vm, vm, vm, pl.BlockSpec(memory_space=pl.ANY)],
        out_specs=vm,
        scratch_shapes=[
            pltpu.VMEM((4, HEAD, 2 * HEAD), bf16),
            pltpu.VMEM((4, HEAD, 2 * HEAD), bf16),
            pltpu.VMEM((HEAD, 2 * HEAD), bf16),
            pltpu.VMEM((rows, HEAD), bf16),
            pltpu.VMEM((BLOCK, w_whole.shape[0]), bf16),
            pltpu.VMEM(w_whole.shape, bf16),
            pltpu.SemaphoreType.DMA,
            pltpu.SemaphoreType.DMA((7,)),
            pltpu.SemaphoreType.DMA((4,)),
            pltpu.SemaphoreType.DMA((4,)),
            pltpu.SemaphoreType.DMA((16,)),
            pltpu.SemaphoreType.DMA((16,)),
        ],
        compiler_params=pltpu.CompilerParams(
            vmem_limit_bytes=48 * 1024 * 1024, collective_id=1, has_side_effects=True
        ),
        cost_estimate=pl.CostEstimate(
            flops=10_000_000_000, bytes_accessed=16 * 1024 * 1024, transcendentals=0
        ),
        name="mix",
    )(ps, qh, oh, gain, w_whole)


def expert_hidden(rows_in, gate_weight, up_weight):
    gate_part = jnp.dot(rows_in, gate_weight[0], preferred_element_type=f32)
    up_part = jnp.dot(rows_in, up_weight[0], preferred_element_type=f32)
    return (jax.nn.silu(gate_part) * up_part).astype(bf16)


def slot_numbers(routes, experts, capacity):
    assigned = routes.reshape(-1)
    onehot = (assigned[:, None] == jnp.arange(experts, dtype=jnp.int32)[None, :]).astype(jnp.int32)
    before = jnp.cumsum(onehot, axis=0) - onehot
    return assigned * capacity + jnp.sum(before * onehot, axis=1)


def body(
    mixer_input_rows,
    mixer_norm_gain,
    query_weight,
    key_weight,
    value_weight,
    write_strength_projection,
    decay_projection,
    head_decay_speed,
    largest_write_strength,
    extra_log_decay,
    head_norm_gain,
    mixer_output_weight,
    expert_input_rows,
    expert_norm_gain,
    routes,
    expert_route_weight,
    gate_weight,
    up_weight,
    down_weight,
):
    w_whole = lax.all_gather(mixer_output_weight, TP, axis=0, tiled=True)
    mix_normed = rms_scale(mixer_input_rows, mixer_norm_gain)
    exp_normed = rms_scale(expert_input_rows, expert_norm_gain)
    token_count, top_count = routes.shape
    model_width = exp_normed.shape[1]
    experts = gate_weight.shape[0] * lax.axis_size(EP)
    capacity = 2
    slot_ids = slot_numbers(routes, experts, capacity)
    places = jnp.arange(experts * capacity, dtype=jnp.int32)
    selector = jnp.sum(
        (slot_ids.reshape(token_count, top_count)[None, :, :] == places[:, None, None]).astype(f32),
        axis=2,
    )
    sending = jnp.dot(
        selector.astype(bf16), exp_normed, preferred_element_type=f32
    ).astype(bf16)
    arrived = lax.all_to_all(
        sending.reshape(experts, capacity, model_width), EP, split_axis=0, concat_axis=0, tiled=True
    )
    arrived = arrived.reshape(-1, model_width)
    ps, qh, oh = span_call(
        lax.all_gather(mix_normed, TP, axis=0, tiled=True),
        query_weight, key_weight, value_weight,
        write_strength_projection, decay_projection,
        head_decay_speed, largest_write_strength, extra_log_decay,
    )
    mix_out = mix_call(ps, qh, oh, head_norm_gain.reshape(1, HEAD), w_whole)
    hidden = expert_hidden(whole_of(arrived, TP, 0), gate_weight, up_weight)
    expert_sum = sum_at_owner(
        jnp.dot(hidden, down_weight[0], preferred_element_type=f32).astype(bf16),
        TP,
        0,
    )
    finished = expert_sum.astype(bf16).reshape(experts, capacity, model_width)
    returned = lax.all_to_all(finished, EP, split_axis=0, concat_axis=0, tiled=True)
    results = returned.reshape(experts * capacity, model_width)[slot_ids].astype(f32)
    results = results.reshape(token_count, top_count, model_width)
    exp_out = jnp.sum(results * expert_route_weight[:, :, None], axis=1).astype(bf16)
    return (mix_out, exp_out)


def solution(mesh):
    torus = Mesh(mesh.devices.reshape(4, 4, 8, 2), ("ep_0", "ep_1", "tp_0", "tp_1"))
    placed = (
        P(EP_TP, None),
        P(),
        P(None, TP),
        P(None, TP),
        P(None, TP),
        P(),
        P(),
        P(TP),
        P(TP),
        P(EP, TP),
        P(),
        P(TP, None),
        P(EP_TP, None),
        P(),
        P(EP_TP, None),
        P(EP_TP, None),
        P(EP, None, TP),
        P(EP, None, TP),
        P(EP, TP, None),
    )
    return jax.shard_map(
        body,
        mesh=torus,
        in_specs=placed,
        out_specs=(P(EP_TP, None), P(EP_TP, None)),
        check_vma=False,
    )
```

time: 567 us -> 270 us (0.48)
  other arithmetic: 180 us -> 6.57 us
  matrix products: 128 us -> 10.1 us
  Pallas kernels: 0 us -> 79.2 us
  blocking collectives: 55.8 us -> 18.1 us
  local copies, waits for them, and re-layouts: 29.8 us -> 10.1 us
  starting transfers between devices: 31.6 us -> 15.8 us
  waiting for transfers between devices: 121 us -> 115 us
    another operation x4 -> x0, other arithmetic: 159 us -> none  [the longest x3 159 us: block_terms(): jax.scipy.linalg.solve_triangular(system, right_side, lower=True, unit_di...]
    dot_general x120 -> x3, matrix products: 126 us -> 10.1 us  [the longest x1 5.84 us: body(): jnp.dot(hidden, down_weight[0], preferred_element_type=f32).astype(bf16)]
    pallas_call x0 -> x2, Pallas kernels: none -> 79.2 us  [the longest x1 47.2 us: span_call(): pl.pallas_call(span_kernel, out_shape=(jax.ShapeDtypeStruct((HEAD, 2 * HE...]
    all_gather x4 -> x0, blocking collectives: 37.8 us -> none  [prefix_by_axis(): lax.all_gather(part.astype(kind), axis)]
    all_to_all x1 -> x0, starting transfers between devices: 15.7 us -> none  [body(): lax.all_to_all(head_outputs_mixed, TP, split_axis=0, concat_axis=1, tiled...]
    all_to_all x1 -> x0, waiting for transfers between devices: 15.4 us -> none  [body(): lax.all_to_all(head_outputs_mixed, TP, split_axis=0, concat_axis=1, tiled...]
    dynamic_slice x19 -> x0, local copies, waits for them, and re-layouts: 10.8 us -> none  [the longest x16 9.4 us: delta_rule_kernel(): _, outputs = lax.scan(advance, entering, terms)]
    another operation x5 -> x0, local copies, waits for them, and re-layouts: 8.34 us -> none  [blocked(): tensor.reshape(block_count, BLOCK, heads_here, -1).transpose(0, 2, 1, 3)]
  transfers between devices with their start and end apart: 6 -> 5, of which waited for: 4 -> 4; matrix products, arithmetic and copies ran while one was open for 56% -> 7% of each run, Pallas kernels for 0% -> 18%
where the time goes in v1:
time: 270 us
  waiting for transfers between devices  115 us (43%)
  Pallas kernels  79.2 us (29%)
  blocking collectives  18.1 us (7%)
  starting transfers between devices  15.8 us (6%)
  between operations  15.2 us (6%)
  local copies, waits for them, and re-layouts  10.1 us (4%)
  matrix products  10.1 us (4%)
  other arithmetic  6.57 us (2%)
    all_to_all x1, waiting for transfers between devices, sum_at_owner(): parts = lax.all_to_all(cut_along(x, dim, devices), axis, 0, 0, tiled=True)  70.6 us
    pallas_call x1, Pallas kernels, span_call(): pl.pallas_call(span_kernel, out_shape=(jax.ShapeDtypeStruct((HEAD, 2 * HE...  47.2 us
    all_gather x1, waiting for transfers between devices, whole_of(): x = lax.all_gather(x, axis, axis=dim, tiled=True)  32.7 us
    pallas_call x1, Pallas kernels, mix_call(): pl.pallas_call(mix_kernel, out_shape=jax.ShapeDtypeStruct((BLOCK, model),...  31.9 us
    all_to_all x1, blocking collectives, body(): lax.all_to_all(sending.reshape(experts, capacity, model_width), EP, split...  14.2 us
    all_to_all x1, starting transfers between devices, sum_at_owner(): parts = lax.all_to_all(cut_along(x, dim, devices), axis, 0, 0, tiled=True)  9.15 us
    all_gather x1, waiting for transfers between devices, body(): w_whole = lax.all_gather(mixer_output_weight, TP, axis=0, tiled=True)  8.27 us
    unnamed x28, local copies, waits for them, and re-layouts  8.16 us
  transfers between devices with their start and end apart: 5, of which 4 were waited for; matrix products, arithmetic and copies ran while one was open for 7% of the time, Pallas kernels for 18%

profile of v1, /device:TPU:1, one launch (start us, length us, event | category | flops | bytes accessed | tf_op | source)
XLA Modules:
  0.0 269.8 jit_solution(8331001809376412969)
XLA Ops:
  7.2 1.0 fusion.17
  9.7 1.0 convolution_convert_fusion.1
  10.8 14.2 %all_to_all.15 = bf16[16,2,2048]{2,1,0:T(2,128)(2,1)S(1)} all-to-all(bf16[16,2,2048]{2,1,0:T(2,128)(2,1)S(1)} %reshape.82), channel_id=1, replica_groups=mesh['ep_0'=4,'ep_1'=4,'tp_0'=8,'tp_1'=2] {'ep_0','ep_1'}, dimensions={0} | all-to-all | bytes 262144 | tf_op jit(solution)/shard_map/all_to_all | solution.py:423
  25.1 3.8 %all_gather.14 = bf16[64,2048]{1,0:T(8,128)(2,1)} all-gather(bf16[32,2048]{1,0:T(8,128)(2,1)S(1)} %reshape.83), channel_id=1, replica_groups=mesh['ep_0'=4,'ep_1'=4,'tp_0'=8,'tp_1'=2] {'tp_1'}, dimensions={0}, use_global_device_ids=true | all-gather | bytes 393216 | tf_op jit(solution)/shard_map/all_gather | solution.py:35
  29.0 1.2 fusion.11
  30.3 1.0 fusion.13
  32.0 32.7 %all-gather.8.cloned.1.call-done = bf16[512,2048]{1,0:T(8,128)(2,1)} async-done(((bf16[64,2048]{1,0:T(8,128)(2,1)}), bf16[512,2048]{1,0:T(8,128)(2,1)}) %all-gather.8.cloned.1.call-update) | async-done | bytes 2097168 | tf_op jit(solution)/shard_map/all_gather | solution.py:35
  64.7 3.3 %fusion.3 = f32[512,448]{0,1:T(8,128)S(1)} fusion(bf16[512,2048]{1,0:T(8,128)(2,1)} %all-gather.8.cloned.1.call-done, bf16[1,2048,448]{1,2,0:T(8,128)(2,1)} %param.35), kind=kOutput, calls=%fused_computation.6 | convolution fusion | flops 939524096 | bytes 4849664 | tf_op jit(solution)/shard_map/dot_general | solution.py:374
  68.0 5.8 %convolution_convert_fusion = bf16[512,2048]{1,0:T(8,128)(2,1)} fusion(bf16[1,448,2048]{2,1,0:T(8,128)(2,1)S(1)} %copy-done, bf16[512,2048]{1,0:T(8,128)(2,1)} %all-gather.8.cloned.1.call-done, bf16[1,2048,448]{1,2,0:T(8,128)(2,1)} %param.36, f32[512,448]{0,1:T(8,128)S(1)} %fusion.3), kind=kOutput, calls=%fused_computation.1 | convolution fusion | flops 1881473024 | bytes 8781824 | tf_op jit(solution)/shard_map/dot_general | solution.py:436
  73.8 9.2 %all-to-all-start.1 = ((bf16[16,32,2048]{2,1,0:T(8,128)(2,1)}), bf16[16,32,2048]{2,1,0:T(8,128)(2,1)}, u32[]{:S(2)}, u32[]{:S(2)}) async-start(bf16[16,32,2048]{2,1,0:T(8,128)(2,1)} %bitcast.27), calls=%async_computation.1 | async-start | bytes 4194304 | tf_op jit(solution)/shard_map/all_to_all | solution.py:47
  83.1 70.6 %all-to-all-done.1 = bf16[16,32,2048]{2,1,0:T(8,128)(2,1)} async-done(((bf16[16,32,2048]{2,1,0:T(8,128)(2,1)}), bf16[16,32,2048]{2,1,0:T(8,128)(2,1)}, u32[]{:S(2)}, u32[]{:S(2)}) %all-to-all-start.1) | async-done | bytes 2097184 | tf_op jit(solution)/shard_map/all_to_all | solution.py:47
  153.7 2.1 reduce_sum.66
  156.5 6.5 %all-to-all-start.2 = ((bf16[16,2,2048]{2,1,0:T(2,128)(2,1)}), bf16[16,2,2048]{2,1,0:T(2,128)(2,1)S(1)}, u32[]{:S(2)}, u32[]{:S(2)}) async-start(bf16[16,2,2048]{2,1,0:T(2,128)(2,1)} %reshape.85), calls=%async_computation.2 | async-start | bytes 262144 | tf_op jit(solution)/shard_map/all_to_all | solution.py:441
  163.1 1.0 copy.33.ws_ref
  164.1 1.0 copy.34.wd_ref
  166.4 1.4 copy.35.extra_ref
  167.9 2.4 all-to-all-done.2
  171.0 0.9 multiply_reduce_fusion
  171.9 47.2 %span.1 = (bf16[128,256]{1,0:T(8,128)(2,1)}, bf16[2048,128]{1,0:T(8,128)(2,1)}, f32[2048,128]{1,0:T(8,128)}) custom-call(bf16[2048,2048]{1,0:T(8,128)(2,1)} %all-gather.4.cloned.1.call-done.x_ref, bf16[2048,128]{1,0:T(8,128)(2,1)} %wq_ref.1, bf16[2048,128]{1,0:T(8,128)(2,1)} %wk_ref.1, bf16[2048,128]{1,0:T(8,128)(2,1)} %wv_ref.1, ...), custom_call_target="tpu_custom_call" | custom-call | flops 30000001024 | bytes 16777216 | tf_op jit(solution)/shard_map/span/pallas_call | solution.py:200
  219.1 8.3 %all-gather.6.cloned.1.call-done.w_ref = bf16[2048,2048]{1,0:T(8,128)(2,1)} async-done(((bf16[128,2048]{1,0:T(8,128)(2,1)}), bf16[2048,2048]{1,0:T(8,128)(2,1)}) %all-gather.6.cloned.1.call-update) | async-done | bytes 8388624 | tf_op jit(solution)/shard_map/all_gather | solution.py:407
  227.4 1.2 copy-done.2
  228.6 1.0 copy-done.3
  229.7 0.8 copy-done.4
  230.5 31.9 %mix.1 = bf16[128,2048]{1,0:T(8,128)(2,1)S(1)} custom-call(bf16[128,256]{1,0:T(8,128)(2,1)S(1)} %copy-done.4, bf16[2048,128]{1,0:T(8,128)(2,1)S(1)} %copy-done.3, f32[2048,128]{1,0:T(8,128)S(1)} %copy-done.2, f32[1,128]{1,0:T(1,128)S(1)} %bitcast.26, bf16[2048,2048]{1,0:T(8,128)(2,1)} %all-gather.6.cloned.1.call-done.w_ref), custom_call_target="tpu_custom_call" | custom-call | flops 10000000000 | bytes 16777216 | tf_op jit(solution)/shard_map/mix/pallas_call | solution.py:344
  (48 shorter events, 4.9 us)
Async XLA Ops:
  7.2 60.8 %copy-start = (bf16[1,448,2048]{2,1,0:T(8,128)(2,1)S(1)}, bf16[1,448,2048]{2,1,0:T(8,128)(2,1)}, u32[]{:S(2)}) copy-start(bf16[1,448,2048]{2,1,0:T(8,128)(2,1)} %param.37) | copy-start | bytes 5505028
  7.2 23.1 %copy-start.5 = (bf16[128,2048]{1,0:T(8,128)(2,1)S(1)}, bf16[128,2048]{1,0:T(8,128)(2,1)}, u32[]{:S(2)}) copy-start(bf16[128,2048]{1,0:T(8,128)(2,1)} %param.19) | copy-start | bytes 1572868
  7.2 23.1 %copy-start.8 = (f32[2048]{0:T(1024)S(1)}, f32[2048]{0:T(1024)}, u32[]{:S(2)}) copy-start(f32[2048]{0:T(1024)} %param.20) | copy-start | bytes 24580
  7.2 57.5 %all-gather.8.cloned.1.call-start = ((), (), s32[]{:S(2)}) async-start(), calls=%async_computation.5 | async-start | bytes 2359296 | tf_op jit(solution)/shard_map/all_gather | solution.py:35
  29.0 142.9 %all-gather.4.cloned.1.call-start = ((), (), s32[]{:S(2)}) async-start(), calls=%async_computation.3 | async-start | bytes 8912896 | tf_op jit(solution)/shard_map/all_gather | solution.py:428
  31.3 196.1 %all-gather.6.cloned.1.call-start = ((), (), s32[]{:S(2)}) async-start(), calls=%async_computation.4 | async-start | bytes 8912896 | tf_op jit(solution)/shard_map/all_gather | solution.py:407
  73.8 79.9 %all-to-all-start.1 = ((bf16[16,32,2048]{2,1,0:T(8,128)(2,1)}), bf16[16,32,2048]{2,1,0:T(8,128)(2,1)}, u32[]{:S(2)}, u32[]{:S(2)}) async-start(bf16[16,32,2048]{2,1,0:T(8,128)(2,1)} %bitcast.27), calls=%async_computation.1 | async-start | bytes 4194304 | tf_op jit(solution)/shard_map/all_to_all | solution.py:47
  83.0 80.1 %copy-start.6 = (bf16[2048,16]{0,1:T(8,128)(2,1)S(1)}, bf16[2048,16]{0,1:T(8,128)(2,1)}, u32[]{:S(2)}) copy-start(bf16[2048,16]{0,1:T(8,128)(2,1)} %param.24) | copy-start | bytes 196612
  83.0 81.1 %copy-start.7 = (bf16[2048,16]{0,1:T(8,128)(2,1)S(1)}, bf16[2048,16]{0,1:T(8,128)(2,1)}, u32[]{:S(2)}) copy-start(bf16[2048,16]{0,1:T(8,128)(2,1)} %param.25) | copy-start | bytes 196612
  83.0 83.4 %copy-start.9 = (f32[2048,1]{0,1:T(1,128)S(1)}, f32[2048,1]{0,1:T(1,128)}, u32[]{:S(2)}) copy-start(f32[2048,1]{0,1:T(1,128)} %param.28) | copy-start | bytes 24580
  83.1 84.7 %copy-start.10 = (f32[8,2]{0,1:T(2,128)S(1)}, f32[8,2]{0,1:T(2,128)}, u32[]{:S(2)}) copy-start(f32[8,2]{0,1:T(2,128)} %param.34) | copy-start | bytes 196
  156.5 13.7 %all-to-all-start.2 = ((bf16[16,2,2048]{2,1,0:T(2,128)(2,1)}), bf16[16,2,2048]{2,1,0:T(2,128)(2,1)S(1)}, u32[]{:S(2)}, u32[]{:S(2)}) async-start(bf16[16,2,2048]{2,1,0:T(2,128)(2,1)} %reshape.85), calls=%async_computation.2 | async-start | bytes 262144 | tf_op jit(solution)/shard_map/all_to_all | solution.py:441
  171.9 55.5 %copy-start.1 = (f32[128]{0:T(128)S(1)}, f32[128]{0:T(128)}, u32[]{:S(2)}) copy-start(f32[128]{0:T(128)} %param.29) | copy-start | bytes 1540
  227.4 1.2 copy-start.2
  228.6 1.0 copy-start.3
  229.7 0.8 copy-start.4
Sparse Core Ops, SparseCore 0:
  29.1 35.5 all-gather.7
  67.1 103.9 all-gather.3
  172.9 54.4 all-gather.5

commit v2 on v0

v2 whole, which is shorter than its diff:
```python
import functools

import jax
import jax.numpy as jnp
from jax import lax
from jax.experimental import pallas as pl
from jax.experimental.pallas import tpu as pltpu
from jax.sharding import Mesh
from jax.sharding import PartitionSpec as P

HEAD = 128
BLOCK = 128
EP = ("ep_0", "ep_1")
TP = ("tp_0", "tp_1")
EP_TP = ("ep_0", "ep_1", "tp_0", "tp_1")
MESH = pl.DeviceIdType.MESH

norm_eps = 1e-06
f32 = jnp.float32
bf16 = jnp.bfloat16


def mm(a, b):
    return jnp.dot(a.astype(bf16), b.astype(bf16), preferred_element_type=f32)


def mm_nt(a, b):
    return lax.dot_general(
        a.astype(bf16), b.astype(bf16), (((1,), (1,)), ((), ())), preferred_element_type=f32
    )


def silu(v):
    return v / (1.0 + jnp.exp(-v))


def project_pair(x, w_all, extra, speed, largest):
    p = jnp.dot(x, w_all, preferred_element_type=f32)
    q = silu(p[:, :HEAD])
    k = silu(p[:, HEAD : 2 * HEAD])
    k = k * lax.rsqrt(jnp.sum(k * k, axis=-1, keepdims=True) + 1e-06)
    v = silu(p[:, 2 * HEAD : 3 * HEAD])
    strength = largest / (1.0 + jnp.exp(-p[:, 3 * HEAD : 4 * HEAD]))
    raw = p[:, 4 * HEAD : 5 * HEAD]
    softplus = jnp.maximum(raw, 0.0) + jnp.log(1.0 + jnp.exp(-jnp.abs(raw)))
    return q, k, v, strength, extra - speed * softplus


def lockstep_invert(systems):
    row = lax.broadcasted_iota(jnp.int32, (BLOCK, BLOCK), 0)
    col = lax.broadcasted_iota(jnp.int32, (BLOCK, BLOCK), 1)
    apart = row ^ col
    eye = jnp.where(row == col, 1.0, 0.0)
    inverses = [eye - jnp.where(apart == 1, a, 0.0) for a in systems]
    size = 2
    while size < BLOCK:
        keep = (apart >= size) & (apart < 4 * size)
        xs = [a.astype(bf16) for a in inverses]
        ns = [mm(x, jnp.where(keep, a, 0.0)).astype(bf16) for x, a in zip(xs, systems)]
        ys = [a - mm(n, x) for a, n, x in zip(inverses, ns, xs)]
        squares = [mm(n, n) for n in ns]
        inverses = [y + mm(n2, y) for y, n2 in zip(ys, squares)]
        size *= 4
    return inverses


def block_maps(qs, ks, vs, strengths, log_decays):
    row = lax.broadcasted_iota(jnp.int32, (BLOCK, BLOCK), 0)
    col = lax.broadcasted_iota(jnp.int32, (BLOCK, BLOCK), 1)
    lower = jnp.where(row >= col, 1.0, 0.0).astype(bf16)
    parts = []
    for a in log_decays:
        high = a.astype(bf16)
        rest = a - high.astype(f32)
        middle = rest.astype(bf16)
        parts.append((high, middle, (rest - middle.astype(f32)).astype(bf16)))
    totals = [mm(lower, h) + mm(lower, m) + mm(lower, l) for h, m, l in parts]
    boths = [mm_nt(jnp.concatenate([q, k], axis=0), k) for q, k in zip(qs, ks)]
    decays = [jnp.exp(jnp.where(row >= col, a - a.T, -1e30)) for a in totals]
    scores = [b[:BLOCK] * d for b, d in zip(boths, decays)]
    systems = [
        jnp.where(row > col, b[BLOCK:] * s * d, 0.0) for b, s, d in zip(boths, strengths, decays)
    ]
    inverses = lockstep_invert(systems)
    growns = [jnp.exp(a) for a in totals]
    rights = [
        jnp.concatenate([s * g * k, s * v], axis=1)
        for s, g, k, v in zip(strengths, growns, ks, vs)
    ]
    solveds = [mm(a, b) for a, b in zip(inverses, rights)]
    lasts = [a[BLOCK - 1 : BLOCK, :] for a in totals]
    lefts = [
        jnp.concatenate([s, (k * jnp.exp(last - a)).T], axis=0)
        for s, k, last, a in zip(scores, ks, lasts, totals)
    ]
    joineds = [mm(a, b) for a, b in zip(lefts, solveds)]
    return [
        (q * g - j[:BLOCK, :HEAD], j[:BLOCK, HEAD:], j[BLOCK:, :HEAD], j[BLOCK:, HEAD:], jnp.exp(last))
        for q, g, j, last in zip(qs, growns, joineds, lasts)
    ]


def pairs_maps(xs, w_all, extras, speed, largest):
    columns = [[], [], [], [], []]
    for x, extra in zip(xs, extras):
        for list_, a in zip(columns, project_pair(x, w_all, extra, speed, largest)):
            list_ += [a[:BLOCK], a[BLOCK:]]
    blocks = block_maps(*columns)
    results = []
    for a, b in zip(blocks[0::2], blocks[1::2]):
        (qa, oa, ga, sa, da), (qb, ob, gb, sb, db) = a, b
        t = mm(jnp.concatenate([gb, qb], axis=0), jnp.concatenate([ga, sa], axis=1))
        g = db * ga + da * gb - t[:BLOCK, :HEAD]
        s = db * sa - t[:BLOCK, HEAD:] + sb
        qb = da * qb - t[BLOCK:, :HEAD]
        ob = t[BLOCK:, HEAD:] + ob
        results.append(
            (jnp.concatenate([qa, qb], axis=0), jnp.concatenate([oa, ob], axis=0), g, s, da * db)
        )
    return results


CHIPS = 8
RING = 4
EPS = RING * RING
SLOTS = 2
ROWS = EPS * SLOTS
MSG = 8


def normed(x, gain):
    widened = x.astype(f32)
    scaled = widened * lax.rsqrt(jnp.mean(widened * widened, axis=-1, keepdims=True) + norm_eps)
    return (scaled * gain).astype(bf16)


def three_parts(a):
    high = a.astype(bf16)
    rest = a - high.astype(f32)
    middle = rest.astype(bf16)
    return high, middle, (rest - middle.astype(f32)).astype(bf16)


def layer_kernel(
    xm_ref, mgain_ref, xe_ref, egain_ref, routes_ref, share_ref, extra_ref, speed_ref, largest_ref,
    hgain_ref, wst_ref, wdt_ref, wq_ref, wk_ref, wv_ref, wo_ref, gate_ref, up_ref, down_ref,
    mix_ref, exp_ref,
    w_all, gate_s, up_s, down_s, xb, eb, lhs_s, g_s, s_s, o_s, d_s, ps_s, qh_s, oh_s,
    row_maps, col_maps, total_s, heads_out, heads_in, wg,
    msg_out, msg_in, pb, pr, ss, rl, ret_out, ret_in,
    load_sem, ring_send, ring_recv, msg_send, msg_recv, ret_send, ret_recv, w_send, w_recv,
    pb_send, pb_recv, rs_send, rs_recv, map_send, row_recv, col_recv, head_send, head_recv,
):
    y, x = lax.axis_index("ep_0"), lax.axis_index("ep_1")
    z, c = lax.axis_index("tp_0"), lax.axis_index("tp_1")
    e = y * RING + x
    t = z * 2 + c
    other = 1 - c

    def at_tp(chip, core):
        return {"tp_0": chip, "tp_1": core}

    def at_ep(o):
        return {"ep_0": o // RING, "ep_1": o % RING}

    def remote(src, dst, send, recv, where):
        return pltpu.make_async_remote_copy(
            src, dst, send, recv, device_id=where, device_id_type=MESH
        )

    loads = [
        pltpu.make_async_copy(wq_ref, w_all.at[:, pl.ds(0, HEAD)], load_sem.at[0]),
        pltpu.make_async_copy(wk_ref, w_all.at[:, pl.ds(HEAD, HEAD)], load_sem.at[1]),
        pltpu.make_async_copy(wv_ref, w_all.at[:, pl.ds(2 * HEAD, HEAD)], load_sem.at[2]),
        pltpu.make_async_copy(gate_ref.at[0], gate_s, load_sem.at[3]),
        pltpu.make_async_copy(up_ref.at[0], up_s, load_sem.at[4]),
        pltpu.make_async_copy(down_ref.at[0], down_s, load_sem.at[5]),
        pltpu.make_async_copy(
            wo_ref.at[:, pl.ds(pl.multiple_of(e * HEAD, HEAD), HEAD)], wg.at[c, e, z], load_sem.at[6]
        ),
    ]
    for copy in loads:
        copy.start()

    barrier = pltpu.get_barrier_semaphore()
    for j in range(1, 16):
        o = (t + j) % 16
        pl.semaphore_signal(barrier, 1, device_id=at_tp(o // 2, o % 2), device_id_type=MESH)
        pl.semaphore_signal(barrier, 1, device_id=at_ep((e + j) % EPS), device_id_type=MESH)

    xb[t] = normed(xm_ref[...], mgain_ref[...])

    lane = lax.broadcasted_iota(jnp.int32, (MSG, 128), 1)
    first = jnp.where(lane // MSG == routes_ref[:, 0:1], 1.0, 0.0)
    second = jnp.where(lane // MSG == routes_ref[:, 1:2], 1.0, 0.0)
    named = first + second
    before = jnp.zeros((MSG, 128), f32)
    token = lax.broadcasted_iota(jnp.int32, (MSG, 128), 0)
    for i in range(MSG - 1):
        before = before + jnp.where(token > i, named[i : i + 1, :], 0.0)
    fills = jnp.where(before == (lane % MSG).astype(f32), named, 0.0)
    shares = fills * (first * share_ref[:, 0:1] + second * share_ref[:, 1:2])
    xn = normed(xe_ref[...], egain_ref[...])
    messages = mm(fills.T, xn)
    for o in range(EPS):
        msg_out[o] = messages[o * MSG : (o + 1) * MSG].astype(bf16)
    pl.semaphore_wait(barrier, 30)

    def ring_copy(block, part, way, where):
        buffer = xb if part == 0 else eb
        return remote(
            buffer.at[block], buffer.at[block], ring_send.at[block, part, way],
            ring_recv.at[block, part], where,
        )

    up_chip, down_chip = (z + 1) % CHIPS, (z + CHIPS - 1) % CHIPS

    def send_own(part):
        ring_copy(t, part, 0, at_tp(up_chip, c)).start()
        ring_copy(t, part, 1, at_tp(down_chip, c)).start()
        ring_copy(t, part, 2, at_tp(z, other)).start()

    def arrived(block, part):
        ring_copy(block, part, 0, at_tp(up_chip, c)).wait_recv()

    send_own(0)
    msg_copies = []
    for j in range(1, EPS):
        o = (e + j) % EPS
        msg_copies.append(
            remote(msg_out.at[o], msg_in.at[e], msg_send.at[j], msg_recv.at[e], at_ep(o))
        )
    for copy in msg_copies:
        copy.start()
    msg_in[e] = msg_out[e]

    heads = wst_ref.shape[0]
    pick = jnp.where(lax.broadcasted_iota(jnp.int32, (heads, HEAD), 0) == t, 1.0, 0.0)
    w_all[:, 3 * HEAD : 4 * HEAD] = mm(wst_ref[...].astype(f32).T, pick).astype(bf16)
    w_all[:, 4 * HEAD : 5 * HEAD] = mm(wdt_ref[...].astype(f32).T, pick).astype(bf16)

    loads[6].wait()
    w_copies = []
    for j in range(1, CHIPS):
        o = (z + j) % CHIPS
        w_copies.append(
            remote(wg.at[c, e, z], wg.at[c, e, z], w_send.at[j], w_recv.at[z], at_tp(o, c))
        )
    for copy in w_copies:
        copy.start()

    for j in range(1, EPS):
        o = (e + j) % EPS
        remote(msg_out.at[0], msg_in.at[o], msg_send.at[0], msg_recv.at[o], at_ep(o)).wait_recv()
    landed = jnp.concatenate([msg_in[o].astype(f32) for o in range(EPS)], axis=0)
    slot = lax.broadcasted_iota(jnp.int32, (ROWS, EPS * MSG), 0)
    line = lax.broadcasted_iota(jnp.int32, (ROWS, EPS * MSG), 1)
    squeeze = jnp.where(
        (line // MSG == slot // SLOTS) & (line % MSG == slot % SLOTS), 1.0, 0.0
    )
    eb[t] = mm(squeeze, landed).astype(bf16)
    for copy in loads[:3]:
        copy.wait()
    send_own(1)

    speed, largest = speed_ref[0], largest_ref[0]

    def extra_of(chip):
        rows = [
            jnp.broadcast_to(extra_ref[chip * 2 + i], (HEAD, BLOCK)).T for i in range(2)
        ]
        return jnp.concatenate(rows, axis=0)

    def span_group(chips):
        xs = [jnp.concatenate([xb[chip * 2], xb[chip * 2 + 1]], axis=0) for chip in chips]
        extras = [extra_of(chip) for chip in chips]
        for chip, (q, o, g, s, d) in zip(chips, pairs_maps(xs, w_all[...], extras, speed, largest)):
            lhs_s[chip, :HEAD] = g.astype(bf16)
            lhs_s[chip, HEAD:] = q.astype(bf16)
            o_s[chip] = o
            g_s[chip] = g
            s_s[chip] = s
            d_s[chip] = jnp.broadcast_to(d, (8, HEAD))

    def pb_copy(chip):
        return remote(
            pb.at[chip, other], pr.at[chip], pb_send.at[chip], pb_recv.at[chip], at_tp(z, other)
        )

    def expert_group(chips):
        rows = jnp.concatenate(
            [eb[chip * 2 + i] for chip in chips for i in range(2)], axis=0
        )
        gated = jnp.dot(rows, gate_s[...], preferred_element_type=f32)
        raised = jnp.dot(rows, up_s[...], preferred_element_type=f32)
        hidden = (silu(gated) * raised).astype(bf16)
        width = 1024
        for n in range(0, down_s.shape[1], width):
            part = jnp.dot(hidden, down_s[:, n : n + width], preferred_element_type=f32)
            for i, chip in enumerate(chips):
                for core in range(2):
                    start = (i * 2 + core) * ROWS
                    pb[chip, core, :, n : n + width] = part[start : start + ROWS].astype(bf16)
        for chip in chips:
            pb_copy(chip).start()

    def rs_copy(chip):
        return remote(ss.at[chip], rl.at[z], rs_send.at[chip], rs_recv.at[z], at_tp(chip, c))

    def add_partner(chip):
        pb_copy(chip).wait_recv()
        ss[chip] = (pb[chip, c].astype(f32) + pr[chip].astype(f32)).astype(bf16)

    arrived(z * 2 + other, 0)
    span_group([z])
    for copy in loads[3:6]:
        copy.wait()
    arrived(z * 2 + other, 1)
    expert_group([z])

    for j in range(1, CHIPS):
        o = (z + j) % CHIPS
        remote(wg.at[c, e, o], wg.at[c, e, o], w_send.at[0], w_recv.at[o], at_tp(o, c)).wait_recv()
    wx_copies = []
    for j in range(1, RING):
        wx_copies.append(
            remote(
                wg.at[c, e], wg.at[c, e], w_send.at[CHIPS + j], w_recv.at[CHIPS + x],
                {"ep_1": (x + j) % RING},
            )
        )
    for copy in wx_copies:
        copy.start()

    def step(k, carry):
        behind, ahead = (z + CHIPS - k) % CHIPS, (z + k) % CHIPS

        def forward(part):
            @pl.when((k < 3) | (c == 0))
            def _():
                ring_copy(behind * 2 + c, part, 0, at_tp(up_chip, c)).start()

            @pl.when((k < 3) | (c == 1))
            def _():
                ring_copy(ahead * 2 + c, part, 1, at_tp(down_chip, c)).start()

        for part in range(2):
            arrived(behind * 2 + c, part)
            arrived(ahead * 2 + c, part)
            forward(part)
            ring_copy(behind * 2 + c, part, 2, at_tp(z, other)).start()
            ring_copy(ahead * 2 + c, part, 2, at_tp(z, other)).start()
            arrived(behind * 2 + other, part)
            arrived(ahead * 2 + other, part)
            if part == 0:
                span_group([behind, ahead])
            else:
                expert_group([behind, ahead])
        return carry

    lax.fori_loop(1, 3, step, 0)
    for j in range(1, RING):
        o = (x + j) % RING
        remote(
            wg.at[c, y * RING + o], wg.at[c, y * RING + o], w_send.at[0], w_recv.at[CHIPS + o],
            {"ep_1": o},
        ).wait_recv()
    wy_copies = []
    for j in range(1, RING):
        line_of = wg.at[c, pl.ds(y * RING, RING)]
        wy_copies.append(
            remote(
                line_of, line_of, w_send.at[CHIPS + RING + j], w_recv.at[CHIPS + RING + y],
                {"ep_0": (y + j) % RING},
            )
        )
    for copy in wy_copies:
        copy.start()
    lax.fori_loop(3, 4, step, 0)

    far = (z + 4) % CHIPS
    for j in range(CHIPS):
        if j != 4:
            chip = (z + j) % CHIPS
            add_partner(chip)
            if j:
                rs_copy(chip).start()
    arrived(far * 2 + c, 0)
    ring_copy(far * 2 + c, 0, 2, at_tp(z, other)).start()
    arrived(far * 2 + other, 0)
    span_group([far])

    g = jnp.zeros((HEAD, HEAD), f32)
    s = jnp.zeros((HEAD, HEAD), f32)
    d = jnp.ones((1, HEAD), f32)
    for chip in range(CHIPS):
        rows = slice(chip * 2 * BLOCK, (chip + 1) * 2 * BLOCK)
        lhs = lhs_s[chip]
        m = mm(lhs, jnp.concatenate([g, s], axis=1))
        qh_s[rows, :] = (d * lhs[HEAD:].astype(f32) - m[HEAD:, :HEAD]).astype(bf16)
        oh_s[rows, :] = m[HEAD:, HEAD:] + o_s[chip]
        dz = d_s[chip, 0:1, :]
        g, s = dz * g + d * g_s[chip] - m[:HEAD, :HEAD], dz * s - m[:HEAD, HEAD:] + s_s[chip]
        d = d * dz
    row = lax.broadcasted_iota(jnp.int32, (HEAD, HEAD), 0)
    col = lax.broadcasted_iota(jnp.int32, (HEAD, HEAD), 1)
    own_map = jnp.concatenate([jnp.where(row == col, d, 0.0) - g, s], axis=1).astype(bf16)
    ps_s[...] = own_map
    map_copies = []
    for j in range(1, RING):
        map_copies.append(
            remote(
                ps_s, row_maps.at[x], map_send.at[j], row_recv.at[x], {"ep_1": (x + j) % RING}
            )
        )
    for copy in map_copies:
        copy.start()
    row_maps[x] = own_map

    arrived(far * 2 + c, 1)
    ring_copy(far * 2 + c, 1, 2, at_tp(z, other)).start()
    arrived(far * 2 + other, 1)
    expert_group([far])

    for j in range(1, RING):
        o = (x + j) % RING
        remote(ps_s, row_maps.at[o], map_send.at[0], row_recv.at[o], {"ep_1": o}).wait_recv()
    whole = row_maps[0]
    mine = whole
    for k in range(1, RING):
        mine = jnp.where(x == k, whole, mine)
        later = row_maps[k]
        m = mm(later[:, :HEAD], whole)
        whole = jnp.concatenate(
            [m[:, :HEAD], m[:, HEAD:] + later[:, HEAD:].astype(f32)], axis=1
        ).astype(bf16)
    total_s[...] = whole
    total_copies = []
    for j in range(1, RING):
        total_copies.append(
            remote(
                total_s, col_maps.at[y], map_send.at[RING + j], col_recv.at[y],
                {"ep_0": (y + j) % RING},
            )
        )
    for copy in total_copies:
        copy.start()
    col_maps[y] = whole

    add_partner(far)
    rs_copy(far).start()
    for j in range(1, RING):
        o = (y + j) % RING
        line_of = wg.at[c, pl.ds(o * RING, RING)]
        remote(
            line_of, line_of, w_send.at[0], w_recv.at[CHIPS + RING + o], {"ep_0": o}
        ).wait_recv()
    w_half = remote(
        wg.at[c], wg.at[c], w_send.at[CHIPS + 2 * RING], w_recv.at[CHIPS + 2 * RING],
        at_tp(z, other),
    )
    w_half.start()

    for j in range(1, RING):
        o = (y + j) % RING
        remote(
            total_s, col_maps.at[o], map_send.at[0], col_recv.at[o], {"ep_0": o}
        ).wait_recv()
    memory = jnp.zeros((HEAD, HEAD), f32)
    for k in range(RING - 1):
        earlier = col_maps[k]
        moved = earlier[:, HEAD:].astype(f32)
        if k:
            moved = moved + mm(earlier[:, :HEAD], memory)
        memory = jnp.where(k < y, moved, memory)
    moved = mm(mine[:, :HEAD], memory) + mine[:, HEAD:].astype(f32)
    memory = jnp.where(x > 0, moved, memory).astype(bf16)

    hgain = hgain_ref[...]
    for chip in range(CHIPS):
        rows = slice(chip * 2 * BLOCK, (chip + 1) * 2 * BLOCK)
        o = mm(qh_s[rows, :], memory) + oh_s[rows, :]
        o = o * lax.rsqrt(jnp.mean(o * o, axis=-1, keepdims=True) + norm_eps)
        heads_out[rows, :] = (o * hgain).astype(bf16)
    own_cols = pl.ds(pl.multiple_of(t * HEAD, HEAD), HEAD)
    head_copies = []
    for j in range(1, 16):
        o = (t + j) % 16
        rows = pl.ds(pl.multiple_of(o * BLOCK, BLOCK), BLOCK)
        head_copies.append(
            remote(
                heads_out.at[rows, :], heads_in.at[:, own_cols], head_send.at[j], head_recv.at[t],
                at_tp(o // 2, o % 2),
            )
        )
    for copy in head_copies:
        copy.start()
    heads_in[:, own_cols] = heads_out[pl.ds(pl.multiple_of(t * BLOCK, BLOCK), BLOCK), :]

    total = ss[z].astype(f32)
    for j in range(1, CHIPS):
        o = (z + j) % CHIPS
        remote(ss.at[0], rl.at[o], rs_send.at[o], rs_recv.at[o], at_tp(o, c)).wait_recv()
        total = total + rl[o].astype(f32)
    spread_line = lax.broadcasted_iota(jnp.int32, (EPS * MSG, ROWS), 0)
    spread_slot = lax.broadcasted_iota(jnp.int32, (EPS * MSG, ROWS), 1)
    spread = jnp.where(
        (spread_line // MSG == spread_slot // SLOTS)
        & (spread_line % MSG == spread_slot % SLOTS),
        1.0,
        0.0,
    )
    returning = mm(spread, total)
    for o in range(EPS):
        ret_out[o] = returning[o * MSG : (o + 1) * MSG].astype(bf16)
    ret_copies = []
    for j in range(1, EPS):
        o = (e + j) % EPS
        ret_copies.append(
            remote(ret_out.at[o], ret_in.at[e], ret_send.at[j], ret_recv.at[e], at_ep(o))
        )
    for copy in ret_copies:
        copy.start()
    ret_in[e] = ret_out[e]

    remote(
        wg.at[other], wg.at[other], w_send.at[0], w_recv.at[CHIPS + 2 * RING], at_tp(z, other)
    ).wait_recv()
    for j in range(1, 16):
        o = (t + j) % 16
        cols = pl.ds(pl.multiple_of(o * HEAD, HEAD), HEAD)
        remote(
            heads_out.at[pl.ds(0, BLOCK), :], heads_in.at[:, cols], head_send.at[0],
            head_recv.at[o], at_tp(o // 2, o % 2),
        ).wait_recv()
    for pair in range(EPS // 2):
        weight = jnp.concatenate(
            [
                jnp.concatenate(
                    [wg[core, 2 * pair + i, chip] for chip in range(CHIPS) for core in range(2)],
                    axis=0,
                )
                for i in range(2)
            ],
            axis=1,
        )
        mix_ref[:, pair * 2 * HEAD : (pair + 1) * 2 * HEAD] = jnp.dot(
            heads_in[...], weight, preferred_element_type=f32
        ).astype(bf16)

    for j in range(1, EPS):
        o = (e + j) % EPS
        remote(ret_out.at[0], ret_in.at[o], ret_send.at[0], ret_recv.at[o], at_ep(o)).wait_recv()
    results = jnp.concatenate([ret_in[o].astype(f32) for o in range(EPS)], axis=0).astype(bf16)
    out = sum(jnp.dot(a, results, preferred_element_type=f32) for a in three_parts(shares))
    exp_ref[...] = out.astype(bf16)

    for copy in (
        msg_copies + w_copies + wx_copies + wy_copies + [w_half] + map_copies + total_copies
        + head_copies + ret_copies
    ):
        copy.wait_send()
    for part in range(2):
        ring_copy(t, part, 0, at_tp(up_chip, c)).wait_send()
        ring_copy(t, part, 1, at_tp(down_chip, c)).wait_send()
        ring_copy(t, part, 2, at_tp(z, other)).wait_send()
        for k in range(1, 4):
            behind, ahead = (z + CHIPS - k) % CHIPS, (z + k) % CHIPS

            @pl.when((k < 3) | (c == 0))
            def _():
                ring_copy(behind * 2 + c, part, 0, at_tp(up_chip, c)).wait_send()

            @pl.when((k < 3) | (c == 1))
            def _():
                ring_copy(ahead * 2 + c, part, 1, at_tp(down_chip, c)).wait_send()

            ring_copy(behind * 2 + c, part, 2, at_tp(z, other)).wait_send()
            ring_copy(ahead * 2 + c, part, 2, at_tp(z, other)).wait_send()
        ring_copy(far * 2 + c, part, 2, at_tp(z, other)).wait_send()
    for chip in range(CHIPS):
        pb_copy(chip).wait_send()
    for j in range(1, CHIPS):
        rs_copy((z + j) % CHIPS).wait_send()


def body(
    mixer_input_rows,
    mixer_norm_gain,
    query_weight,
    key_weight,
    value_weight,
    write_strength_projection,
    decay_projection,
    head_decay_speed,
    largest_write_strength,
    extra_log_decay,
    head_norm_gain,
    mixer_output_weight,
    expert_input_rows,
    expert_norm_gain,
    routes,
    expert_route_weight,
    gate_weight,
    up_weight,
    down_weight,
):
    rows, model = mixer_input_rows.shape
    tokens = expert_input_rows.shape[0]
    hidden = gate_weight.shape[2]
    span = extra_log_decay.shape[0]
    blocks = span // BLOCK
    vm = pl.BlockSpec(memory_space=pltpu.VMEM)
    sm = pl.BlockSpec(memory_space=pltpu.SMEM)
    hbm = pl.BlockSpec(memory_space=pl.ANY)
    dma = pltpu.SemaphoreType.DMA
    return pl.pallas_call(
        layer_kernel,
        out_shape=(
            jax.ShapeDtypeStruct((rows, model), bf16),
            jax.ShapeDtypeStruct((tokens, model), bf16),
        ),
        in_specs=[vm] * 7 + [sm] * 2 + [vm] * 3 + [hbm] * 7,
        out_specs=(vm, vm),
        scratch_shapes=[
            pltpu.VMEM((model, 5 * HEAD), bf16),
            pltpu.VMEM((model, hidden), bf16),
            pltpu.VMEM((model, hidden), bf16),
            pltpu.VMEM((hidden, model), bf16),
            pltpu.VMEM((blocks, BLOCK, model), bf16),
            pltpu.VMEM((blocks, ROWS, model), bf16),
            pltpu.VMEM((CHIPS, 3 * HEAD, HEAD), bf16),
            pltpu.VMEM((CHIPS, HEAD, HEAD), f32),
            pltpu.VMEM((CHIPS, HEAD, HEAD), f32),
            pltpu.VMEM((CHIPS, 2 * BLOCK, HEAD), f32),
            pltpu.VMEM((CHIPS, 8, HEAD), f32),
            pltpu.VMEM((HEAD, 2 * HEAD), bf16),
            pltpu.VMEM((span, HEAD), bf16),
            pltpu.VMEM((span, HEAD), f32),
            pltpu.VMEM((RING, HEAD, 2 * HEAD), bf16),
            pltpu.VMEM((RING, HEAD, 2 * HEAD), bf16),
            pltpu.VMEM((HEAD, 2 * HEAD), bf16),
            pltpu.VMEM((span, HEAD), bf16),
            pltpu.VMEM((BLOCK, model), bf16),
            pltpu.VMEM((2, EPS, CHIPS, HEAD, HEAD), bf16),
            pltpu.VMEM((EPS, MSG, model), bf16),
            pltpu.VMEM((EPS, MSG, model), bf16),
            pltpu.VMEM((CHIPS, 2, ROWS, model), bf16),
            pltpu.VMEM((CHIPS, ROWS, model), bf16),
            pltpu.VMEM((CHIPS, ROWS, model), bf16),
            pltpu.VMEM((CHIPS, ROWS, model), bf16),
            pltpu.VMEM((EPS, MSG, model), bf16),
            pltpu.VMEM((EPS, MSG, model), bf16),
            dma((7,)),
            dma((16, 2, 3)),
            dma((16, 2)),
            dma((EPS,)),
            dma((EPS,)),
            dma((EPS,)),
            dma((EPS,)),
            dma((CHIPS + 2 * RING + 1,)),
            dma((CHIPS + 2 * RING + 1,)),
            dma((CHIPS,)),
            dma((CHIPS,)),
            dma((CHIPS,)),
            dma((CHIPS,)),
            dma((2 * RING,)),
            dma((RING,)),
            dma((RING,)),
            dma((16,)),
            dma((16,)),
        ],
        compiler_params=pltpu.CompilerParams(
            vmem_limit_bytes=60 * 1024 * 1024, collective_id=1, has_side_effects=True
        ),
        cost_estimate=pl.CostEstimate(
            flops=10_000_000_000, bytes_accessed=32 * 1024 * 1024, transcendentals=0
        ),
        name="layer",
    )(
        mixer_input_rows, mixer_norm_gain.reshape(1, model), expert_input_rows,
        expert_norm_gain.reshape(1, model), routes, expert_route_weight,
        extra_log_decay.reshape(blocks, 1, BLOCK), head_decay_speed, largest_write_strength,
        head_norm_gain.reshape(1, HEAD), write_strength_projection.T, decay_projection.T,
        query_weight, key_weight, value_weight, mixer_output_weight, gate_weight, up_weight,
        down_weight,
    )


def solution(mesh):
    torus = Mesh(mesh.devices.reshape(4, 4, 8, 2), ("ep_0", "ep_1", "tp_0", "tp_1"))
    placed = (
        P(EP_TP, None),
        P(),
        P(None, TP),
        P(None, TP),
        P(None, TP),
        P(),
        P(),
        P(TP),
        P(TP),
        P(EP, TP),
        P(),
        P(TP, None),
        P(EP_TP, None),
        P(),
        P(EP_TP, None),
        P(EP_TP, None),
        P(EP, None, TP),
        P(EP, None, TP),
        P(EP, TP, None),
    )
    return jax.shard_map(
        body,
        mesh=torus,
        in_specs=placed,
        out_specs=(P(EP_TP, None), P(EP_TP, None)),
        check_vma=False,
    )
```

time: 567 us -> 138 us (0.24)
  other arithmetic: 180 us -> 0 us
  matrix products: 128 us -> 0 us
  Pallas kernels: 0 us -> 124 us
  waiting for transfers between devices: 121 us -> 0 us
  blocking collectives: 55.8 us -> 0 us
  starting transfers between devices: 31.6 us -> 0 us
  local copies, waits for them, and re-layouts: 29.8 us -> 12.3 us
  between operations: 15.5 us -> 1.93 us
    another operation x5 -> x0, other arithmetic: 159 us -> none  [the longest x3 159 us: block_terms(): jax.scipy.linalg.solve_triangular(system, right_side, lower=True, unit_di...]
    dot_general x120 -> x0, matrix products: 126 us -> none  [the longest x26 18.6 us: compose(): jnp.einsum('hij,hjk->hik', second_map, first_shift, precision=highest)]
    pallas_call x0 -> x1, Pallas kernels: none -> 124 us  [body(): pl.pallas_call(layer_kernel, out_shape=(jax.ShapeDtypeStruct((rows, model...]
    all_to_all x3 -> x0, waiting for transfers between devices: 78.5 us -> none  [the longest x1 63.1 us: sum_at_owner(): parts = lax.all_to_all(cut_along(x, dim, devices), axis, 0, 0, tiled=True)]
    all_gather x3 -> x0, waiting for transfers between devices: 42.3 us -> none  [the longest x1 34.4 us: whole_of(): x = lax.all_gather(x, axis, axis=dim, tiled=True)]
    all_gather x5 -> x0, blocking collectives: 41.6 us -> none  [the longest x4 37.8 us: prefix_by_axis(): lax.all_gather(part.astype(kind), axis)]
    all_to_all x3 -> x0, starting transfers between devices: 31.5 us -> none  [the longest x1 15.7 us: body(): lax.all_to_all(head_outputs_mixed, TP, split_axis=0, concat_axis=1, tiled...]
    all_to_all x1 -> x0, blocking collectives: 14.2 us -> none  [body(): lax.all_to_all(sending.reshape(experts, capacity, model_width), EP, split...]
  transfers between devices with their start and end apart: 6 -> 0, of which waited for: 4 -> 0; matrix products, arithmetic and copies ran while one was open for 56% -> 0% of each run, Pallas kernels for 0% -> 0%
where the time goes in v2:
time: 138 us
  Pallas kernels  124 us (90%)
  local copies, waits for them, and re-layouts  12.3 us (9%)
  between operations  1.93 us (1%)
    pallas_call x1, Pallas kernels, body(): pl.pallas_call(layer_kernel, out_shape=(jax.ShapeDtypeStruct((rows, model...  124 us
    unnamed x8, local copies, waits for them, and re-layouts  12.3 us

profile of v2, /device:TPU:1, one launch (start us, length us, event | category | flops | bytes accessed | tf_op | source)
XLA Modules:
  0.0 137.9 jit_solution(12105735712941472072)
XLA Ops:
  1.9 1.3 copy.21.routes_ref
  3.3 1.3 copy.22.share_ref
  4.6 0.0 copy-start
  4.6 4.0 %copy.23.gate_ref = bf16[1,2048,448]{2,1,0:T(8,128)(2,1)} copy(bf16[1,2048,448]{1,2,0:T(8,128)(2,1)} %param.35) | data formatting | bytes 3670016 | tf_op args[16]
  8.6 0.0 copy-done
  8.6 2.4 %copy.24.up_ref = bf16[1,2048,448]{2,1,0:T(8,128)(2,1)} copy(bf16[1,2048,448]{1,2,0:T(8,128)(2,1)S(1)} %copy-done) | data formatting | bytes 3670016 | tf_op args[17]
  11.0 123.7 %layer.1 = (bf16[128,2048]{1,0:T(8,128)(2,1)}, bf16[8,2048]{1,0:T(8,128)(2,1)}) custom-call(bf16[128,2048]{1,0:T(8,128)(2,1)} %xm_ref.1, f32[1,2048]{1,0:T(1,128)} %bitcast.8, bf16[8,2048]{1,0:T(8,128)(2,1)} %xe_ref.1, f32[1,2048]{1,0:T(1,128)} %bitcast.9, s32[8,2]{1,0:T(8,128)} %copy.21.routes_ref, f32[8,2]{1,0:T(8,128)} %copy.22.share_ref, ...), custom_call_target="tpu_custom_call" | custom-call | flops 10000000000 | bytes 33554432 | tf_op jit(solution)/shard_map/layer/pallas_call | solution.py:617
  134.7 1.9 %copy.29 = bf16[128,2048]{1,0:T(8,128)(2,1)} copy(bf16[128,2048]{1,0:T(8,128)(2,1)} %get-tuple-element.4) | data formatting | bytes 1048576
  136.6 1.4 copy.30
Async XLA Ops:
  4.6 4.0 %copy-start = (bf16[1,2048,448]{1,2,0:T(8,128)(2,1)S(1)}, bf16[1,2048,448]{1,2,0:T(8,128)(2,1)}, u32[]{:S(2)}) copy-start(bf16[1,2048,448]{1,2,0:T(8,128)(2,1)} %param.36) | copy-start | bytes 5505028

commit v3 on v2

--- a/solution.py
+++ b/solution.py
@@ -156,6 +156,8 @@
     e = y * RING + x
     t = z * 2 + c
     other = 1 - c
+    a, b = jnp.where(c == 0, y, x), jnp.where(c == 0, x, y)
+    f = a * RING + b
 
     def at_tp(chip, core):
         return {"tp_0": chip, "tp_1": core}
@@ -176,7 +178,7 @@
         pltpu.make_async_copy(up_ref.at[0], up_s, load_sem.at[4]),
         pltpu.make_async_copy(down_ref.at[0], down_s, load_sem.at[5]),
         pltpu.make_async_copy(
-            wo_ref.at[:, pl.ds(pl.multiple_of(e * HEAD, HEAD), HEAD)], wg.at[c, e, z], load_sem.at[6]
+            wo_ref.at[:, pl.ds(pl.multiple_of(e * HEAD, HEAD), HEAD)], wg.at[c, f, z], load_sem.at[6]
         ),
     ]
     for copy in loads:
@@ -190,27 +192,32 @@
 
     xb[t] = normed(xm_ref[...], mgain_ref[...])
 
-    lane = lax.broadcasted_iota(jnp.int32, (MSG, 128), 1)
-    first = jnp.where(lane // MSG == routes_ref[:, 0:1], 1.0, 0.0)
-    second = jnp.where(lane // MSG == routes_ref[:, 1:2], 1.0, 0.0)
+    place = lax.broadcasted_iota(jnp.int32, (EPS * MSG, MSG), 0)
+    first = jnp.where(place // MSG == routes_ref[0:1, :], 1.0, 0.0)
+    second = jnp.where(place // MSG == routes_ref[1:2, :], 1.0, 0.0)
     named = first + second
-    before = jnp.zeros((MSG, 128), f32)
-    token = lax.broadcasted_iota(jnp.int32, (MSG, 128), 0)
+    token = lax.broadcasted_iota(jnp.int32, (EPS * MSG, MSG), 1)
+    before = jnp.zeros((EPS * MSG, MSG), f32)
     for i in range(MSG - 1):
-        before = before + jnp.where(token > i, named[i : i + 1, :], 0.0)
-    fills = jnp.where(before == (lane % MSG).astype(f32), named, 0.0)
-    shares = fills * (first * share_ref[:, 0:1] + second * share_ref[:, 1:2])
+        before = before + jnp.where(token > i, named[:, i : i + 1], 0.0)
+    fills = jnp.where(before == (place % MSG).astype(f32), named, 0.0)
+    shares = (fills * (first * share_ref[0:1, :] + second * share_ref[1:2, :])).T
     xn = normed(xe_ref[...], egain_ref[...])
-    messages = mm(fills.T, xn)
+    messages = mm(fills, xn)
     for o in range(EPS):
         msg_out[o] = messages[o * MSG : (o + 1) * MSG].astype(bf16)
     pl.semaphore_wait(barrier, 30)
 
     def ring_copy(block, part, way, where):
-        buffer = xb if part == 0 else eb
+        half = BLOCK // 2
+        piece = (
+            xb.at[block, pl.ds(0, half)],
+            xb.at[block, pl.ds(half, half)],
+            eb.at[block],
+            wg.at[c, f, block // 2],
+        )[part]
         return remote(
-            buffer.at[block], buffer.at[block], ring_send.at[block, part, way],
-            ring_recv.at[block, part], where,
+            piece, piece, ring_send.at[block, part, way], ring_recv.at[block, part], where
         )
 
     up_chip, down_chip = (z + 1) % CHIPS, (z + CHIPS - 1) % CHIPS
@@ -218,11 +225,33 @@
     def send_own(part):
         ring_copy(t, part, 0, at_tp(up_chip, c)).start()
         ring_copy(t, part, 1, at_tp(down_chip, c)).start()
-        ring_copy(t, part, 2, at_tp(z, other)).start()
+        if part < 3:
+            ring_copy(t, part, 2, at_tp(z, other)).start()
 
     def arrived(block, part):
         ring_copy(block, part, 0, at_tp(up_chip, c)).wait_recv()
 
+    def relay(k, part):
+        behind, ahead = (z + CHIPS - k) % CHIPS, (z + k) % CHIPS
+        arrived(behind * 2 + c, part)
+
+        @pl.when((k < 3) | (c == 0))
+        def _():
+            ring_copy(behind * 2 + c, part, 0, at_tp(up_chip, c)).start()
+
+        if part < 3:
+            ring_copy(behind * 2 + c, part, 2, at_tp(z, other)).start()
+        arrived(ahead * 2 + c, part)
+
+        @pl.when((k < 3) | (c == 1))
+        def _():
+            ring_copy(ahead * 2 + c, part, 1, at_tp(down_chip, c)).start()
+
+        if part < 3:
+            ring_copy(ahead * 2 + c, part, 2, at_tp(z, other)).start()
+
+    loads[6].wait()
+    send_own(3)
     send_own(0)
     msg_copies = []
     for j in range(1, EPS):
@@ -239,15 +268,8 @@
     w_all[:, 3 * HEAD : 4 * HEAD] = mm(wst_ref[...].astype(f32).T, pick).astype(bf16)
     w_all[:, 4 * HEAD : 5 * HEAD] = mm(wdt_ref[...].astype(f32).T, pick).astype(bf16)
 
-    loads[6].wait()
-    w_copies = []
-    for j in range(1, CHIPS):
-        o = (z + j) % CHIPS
-        w_copies.append(
-            remote(wg.at[c, e, z], wg.at[c, e, z], w_send.at[j], w_recv.at[z], at_tp(o, c))
-        )
-    for copy in w_copies:
-        copy.start()
+    relay(1, 3)
+    send_own(1)
 
     for j in range(1, EPS):
         o = (e + j) % EPS
@@ -261,7 +283,7 @@
     eb[t] = mm(squeeze, landed).astype(bf16)
     for copy in loads[:3]:
         copy.wait()
-    send_own(1)
+    send_own(2)
 
     speed, largest = speed_ref[0], largest_ref[0]
 
@@ -291,8 +313,8 @@
         rows = jnp.concatenate(
             [eb[chip * 2 + i] for chip in chips for i in range(2)], axis=0
         )
-        gated = jnp.dot(rows, gate_s[...], preferred_element_type=f32)
-        raised = jnp.dot(rows, up_s[...], preferred_element_type=f32)
+        gated = mm_nt(rows, gate_s[...])
+        raised = mm_nt(rows, up_s[...])
         hidden = (silu(gated) * raised).astype(bf16)
         width = 1024
         for n in range(0, down_s.shape[1], width):
@@ -312,82 +334,82 @@
         ss[chip] = (pb[chip, c].astype(f32) + pr[chip].astype(f32)).astype(bf16)
 
     arrived(z * 2 + other, 0)
+    arrived(z * 2 + other, 1)
     span_group([z])
+    relay(2, 3)
     for copy in loads[3:6]:
         copy.wait()
-    arrived(z * 2 + other, 1)
+    arrived(z * 2 + other, 2)
     expert_group([z])
 
-    for j in range(1, CHIPS):
-        o = (z + j) % CHIPS
-        remote(wg.at[c, e, o], wg.at[c, e, o], w_send.at[0], w_recv.at[o], at_tp(o, c)).wait_recv()
-    wx_copies = []
-    for j in range(1, RING):
-        wx_copies.append(
-            remote(
-                wg.at[c, e], wg.at[c, e], w_send.at[CHIPS + j], w_recv.at[CHIPS + x],
-                {"ep_1": (x + j) % RING},
-            )
-        )
-    for copy in wx_copies:
-        copy.start()
-
-    def step(k, carry):
+    def w_copy(stage, side, take):
+        moved = (1 if side == 0 else RING - 1)
+        if stage < 2:
+            ta, tb = a, (b + moved) % RING
+        else:
+            ta, tb = (a + moved) % RING, b
+        where = {"ep_0": jnp.where(c == 0, ta, tb), "ep_1": jnp.where(c == 0, tb, ta)}
+        index = CHIPS + 2 * stage + side
+        return remote(take, take, w_send.at[index], w_recv.at[index], where)
+
+    def w_piece(stage, side, sender):
+        half = CHIPS // 2
+        if stage == 0:
+            return wg.at[c, a * RING + (b + sender) % RING]
+        if stage == 1:
+            source = (b + sender + (RING - 1 if side == 0 else 1)) % RING
+            return wg.at[c, a * RING + source, pl.ds(side * half, half)]
+        if stage == 2:
+            return wg.at[c, pl.ds((a + sender) % RING * RING, RING)]
+        source = (a + sender + (RING - 1 if side == 0 else 1)) % RING
+        return wg.at[c, pl.ds(source * RING + side * (RING // 2), RING // 2)]
+
+    def w_send_stage(stage):
+        for side in range(2):
+            w_copy(stage, side, w_piece(stage, side, 0)).start()
+
+    def w_wait_stage(stage):
+        for side in range(2):
+            sender = RING - 1 if side == 0 else 1
+            w_copy(stage, side, w_piece(stage, side, sender)).wait_recv()
+
+    far = (z + 4) % CHIPS
+
+    for k in range(1, 4):
         behind, ahead = (z + CHIPS - k) % CHIPS, (z + k) % CHIPS
-
-        def forward(part):
-            @pl.when((k < 3) | (c == 0))
-            def _():
-                ring_copy(behind * 2 + c, part, 0, at_tp(up_chip, c)).start()
-
-            @pl.when((k < 3) | (c == 1))
-            def _():
-                ring_copy(ahead * 2 + c, part, 1, at_tp(down_chip, c)).start()
-
-        for part in range(2):
-            arrived(behind * 2 + c, part)
-            arrived(ahead * 2 + c, part)
-            forward(part)
-            ring_copy(behind * 2 + c, part, 2, at_tp(z, other)).start()
-            ring_copy(ahead * 2 + c, part, 2, at_tp(z, other)).start()
-            arrived(behind * 2 + other, part)
-            arrived(ahead * 2 + other, part)
-            if part == 0:
-                span_group([behind, ahead])
-            else:
-                expert_group([behind, ahead])
-        return carry
-
-    lax.fori_loop(1, 3, step, 0)
-    for j in range(1, RING):
-        o = (x + j) % RING
-        remote(
-            wg.at[c, y * RING + o], wg.at[c, y * RING + o], w_send.at[0], w_recv.at[CHIPS + o],
-            {"ep_1": o},
-        ).wait_recv()
-    wy_copies = []
-    for j in range(1, RING):
-        line_of = wg.at[c, pl.ds(y * RING, RING)]
-        wy_copies.append(
-            remote(
-                line_of, line_of, w_send.at[CHIPS + RING + j], w_recv.at[CHIPS + RING + y],
-                {"ep_0": (y + j) % RING},
-            )
-        )
-    for copy in wy_copies:
-        copy.start()
-    lax.fori_loop(3, 4, step, 0)
-
-    far = (z + 4) % CHIPS
+        relay(k, 0)
+        relay(k, 1)
+        for chip in (behind, ahead):
+            for part in range(2):
+                arrived(chip * 2 + other, part)
+        span_group([behind, ahead])
+        relay(k, 2)
+        if k == 1:
+            relay(3, 3)
+        if k == 2:
+            arrived(far * 2 + c, 3)
+            w_send_stage(0)
+        if k == 3:
+            w_wait_stage(1)
+            w_send_stage(2)
+        for chip in (behind, ahead):
+            arrived(chip * 2 + other, 2)
+        expert_group([behind, ahead])
+        if k == 2:
+            w_wait_stage(0)
+            w_send_stage(1)
+
     for j in range(CHIPS):
         if j != 4:
             chip = (z + j) % CHIPS
             add_partner(chip)
             if j:
                 rs_copy(chip).start()
-    arrived(far * 2 + c, 0)
-    ring_copy(far * 2 + c, 0, 2, at_tp(z, other)).start()
-    arrived(far * 2 + other, 0)
+    for part in range(2):
+        arrived(far * 2 + c, part)
+        ring_copy(far * 2 + c, part, 2, at_tp(z, other)).start()
+    for part in range(2):
+        arrived(far * 2 + other, part)
     span_group([far])
 
     g = jnp.zeros((HEAD, HEAD), f32)
@@ -416,10 +438,12 @@
     for copy in map_copies:
         copy.start()
     row_maps[x] = own_map
-
-    arrived(far * 2 + c, 1)
-    ring_copy(far * 2 + c, 1, 2, at_tp(z, other)).start()
-    arrived(far * 2 + other, 1)
+    w_wait_stage(2)
+    w_send_stage(3)
+
+    arrived(far * 2 + c, 2)
+    ring_copy(far * 2 + c, 2, 2, at_tp(z, other)).start()
+    arrived(far * 2 + other, 2)
     expert_group([far])
 
     for j in range(1, RING):
@@ -449,17 +473,6 @@
 
     add_partner(far)
     rs_copy(far).start()
-    for j in range(1, RING):
-        o = (y + j) % RING
-        line_of = wg.at[c, pl.ds(o * RING, RING)]
-        remote(
-            line_of, line_of, w_send.at[0], w_recv.at[CHIPS + RING + o], {"ep_0": o}
-        ).wait_recv()
-    w_half = remote(
-        wg.at[c], wg.at[c], w_send.at[CHIPS + 2 * RING], w_recv.at[CHIPS + 2 * RING],
-        at_tp(z, other),
-    )
-    w_half.start()
 
     for j in range(1, RING):
         o = (y + j) % RING
@@ -475,6 +488,13 @@
         memory = jnp.where(k < y, moved, memory)
     moved = mm(mine[:, :HEAD], memory) + mine[:, HEAD:].astype(f32)
     memory = jnp.where(x > 0, moved, memory).astype(bf16)
+
+    w_wait_stage(3)
+    w_half = remote(
+        wg.at[c], wg.at[c], w_send.at[CHIPS + 8], w_recv.at[CHIPS + 8],
+        at_tp(z, other),
+    )
+    w_half.start()
 
     hgain = hgain_ref[...]
     for chip in range(CHIPS):
@@ -524,7 +544,7 @@
     ret_in[e] = ret_out[e]
 
     remote(
-        wg.at[other], wg.at[other], w_send.at[0], w_recv.at[CHIPS + 2 * RING], at_tp(z, other)
+        wg.at[other], wg.at[other], w_send.at[0], w_recv.at[CHIPS + 8], at_tp(z, other)
     ).wait_recv()
     for j in range(1, 16):
         o = (t + j) % 16
@@ -533,11 +553,18 @@
             heads_out.at[pl.ds(0, BLOCK), :], heads_in.at[:, cols], head_send.at[0],
             head_recv.at[o], at_tp(o // 2, o % 2),
         ).wait_recv()
+    def piece(core, o):
+        return o if core == 0 else o % RING * RING + o // RING
+
     for pair in range(EPS // 2):
         weight = jnp.concatenate(
             [
                 jnp.concatenate(
-                    [wg[core, 2 * pair + i, chip] for chip in range(CHIPS) for core in range(2)],
+                    [
+                        wg[core, piece(core, 2 * pair + i), chip]
+                        for chip in range(CHIPS)
+                        for core in range(2)
+                    ],
                     axis=0,
                 )
                 for i in range(2)
@@ -556,14 +583,13 @@
     exp_ref[...] = out.astype(bf16)
 
     for copy in (
-        msg_copies + w_copies + wx_copies + wy_copies + [w_half] + map_copies + total_copies
+        msg_copies + [w_half] + map_copies + total_copies
         + head_copies + ret_copies
     ):
         copy.wait_send()
-    for part in range(2):
+    for part in range(4):
         ring_copy(t, part, 0, at_tp(up_chip, c)).wait_send()
         ring_copy(t, part, 1, at_tp(down_chip, c)).wait_send()
-        ring_copy(t, part, 2, at_tp(z, other)).wait_send()
         for k in range(1, 4):
             behind, ahead = (z + CHIPS - k) % CHIPS, (z + k) % CHIPS
 
@@ -575,9 +601,12 @@
             def _():
                 ring_copy(ahead * 2 + c, part, 1, at_tp(down_chip, c)).wait_send()
 
-            ring_copy(behind * 2 + c, part, 2, at_tp(z, other)).wait_send()
-            ring_copy(ahead * 2 + c, part, 2, at_tp(z, other)).wait_send()
-        ring_copy(far * 2 + c, part, 2, at_tp(z, other)).wait_send()
+        if part < 3:
+            for j in range(CHIPS):
+                ring_copy((z + j) % CHIPS * 2 + c, part, 2, at_tp(z, other)).wait_send()
+    for stage in range(4):
+        for side in range(2):
+            w_copy(stage, side, w_piece(stage, side, 0)).wait_send()
     for chip in range(CHIPS):
         pb_copy(chip).wait_send()
     for j in range(1, CHIPS):
@@ -612,7 +641,7 @@
     blocks = span // BLOCK
     vm = pl.BlockSpec(memory_space=pltpu.VMEM)
     sm = pl.BlockSpec(memory_space=pltpu.SMEM)
-    hbm = pl.BlockSpec(memory_space=pl.ANY)
+    hbm = pl.BlockSpec(memory_space=pltpu.HBM)
     dma = pltpu.SemaphoreType.DMA
     return pl.pallas_call(
         layer_kernel,
@@ -624,8 +653,8 @@
         out_specs=(vm, vm),
         scratch_shapes=[
             pltpu.VMEM((model, 5 * HEAD), bf16),
-            pltpu.VMEM((model, hidden), bf16),
-            pltpu.VMEM((model, hidden), bf16),
+            pltpu.VMEM((hidden, model), bf16),
+            pltpu.VMEM((hidden, model), bf16),
             pltpu.VMEM((hidden, model), bf16),
             pltpu.VMEM((blocks, BLOCK, model), bf16),
             pltpu.VMEM((blocks, ROWS, model), bf16),
@@ -652,14 +681,14 @@
             pltpu.VMEM((EPS, MSG, model), bf16),
             pltpu.VMEM((EPS, MSG, model), bf16),
             dma((7,)),
-            dma((16, 2, 3)),
-            dma((16, 2)),
+            dma((16, 4, 3)),
+            dma((16, 4)),
             dma((EPS,)),
             dma((EPS,)),
             dma((EPS,)),
             dma((EPS,)),
-            dma((CHIPS + 2 * RING + 1,)),
-            dma((CHIPS + 2 * RING + 1,)),
+            dma((CHIPS + 9,)),
+            dma((CHIPS + 9,)),
             dma((CHIPS,)),
             dma((CHIPS,)),
             dma((CHIPS,)),
@@ -679,11 +708,11 @@
         name="layer",
     )(
         mixer_input_rows, mixer_norm_gain.reshape(1, model), expert_input_rows,
-        expert_norm_gain.reshape(1, model), routes, expert_route_weight,
+        expert_norm_gain.reshape(1, model), routes.T, expert_route_weight.T,
         extra_log_decay.reshape(blocks, 1, BLOCK), head_decay_speed, largest_write_strength,
         head_norm_gain.reshape(1, HEAD), write_strength_projection.T, decay_projection.T,
-        query_weight, key_weight, value_weight, mixer_output_weight, gate_weight, up_weight,
-        down_weight,
+        query_weight, key_weight, value_weight, mixer_output_weight,
+        jnp.swapaxes(gate_weight, 1, 2), jnp.swapaxes(up_weight, 1, 2), down_weight,
     )
 
 

time: 138 us -> 113 us (0.82)
  Pallas kernels: 124 us -> 108 us
  local copies, waits for them, and re-layouts: 12.3 us -> 3.26 us
    pallas_call x1, Pallas kernels: 124 us -> 108 us  [body(): pl.pallas_call(layer_kernel, out_shape=(jax.ShapeDtypeStruct((rows, model...]
    unnamed x8 -> x2, local copies, waits for them, and re-layouts: 12.3 us -> 3.26 us
where the time goes in v3:
time: 113 us
  Pallas kernels  108 us (96%)
  local copies, waits for them, and re-layouts  3.26 us (3%)
  between operations  1.94 us (2%)
    pallas_call x1, Pallas kernels, body(): pl.pallas_call(layer_kernel, out_shape=(jax.ShapeDtypeStruct((rows, model...  108 us
    unnamed x2, local copies, waits for them, and re-layouts  3.26 us

profile of v3, /device:TPU:1, one launch (start us, length us, event | category | flops | bytes accessed | tf_op | source)
XLA Modules:
  0.0 112.8 jit_solution(2783383799739776528)
XLA Ops:
  1.9 107.6 %layer.1 = (bf16[128,2048]{1,0:T(8,128)(2,1)}, bf16[8,2048]{1,0:T(8,128)(2,1)}) custom-call(bf16[128,2048]{1,0:T(8,128)(2,1)} %xm_ref.1, f32[1,2048]{1,0:T(1,128)} %bitcast.14, bf16[8,2048]{1,0:T(8,128)(2,1)} %xe_ref.1, f32[1,2048]{1,0:T(1,128)} %bitcast.15, s32[2,8]{1,0:T(2,128)} %bitcast.17, f32[2,8]{1,0:T(2,128)} %bitcast.18, f32[16,1,128]{2,1,0:T(1,128)} %bitcast.16, ...), custom_call_target="tpu_custom_call" | custom-call | flops 10000000000 | bytes 33554432 | tf_op jit(solution)/shard_map/layer/pallas_call | solution.py:646
  109.5 1.9 %copy.25 = bf16[128,2048]{1,0:T(8,128)(2,1)} copy(bf16[128,2048]{1,0:T(8,128)(2,1)} %get-tuple-element.4) | data formatting | bytes 1048576
  111.4 1.4 %copy.26 = bf16[8,2048]{1,0:T(8,128)(2,1)} copy(bf16[8,2048]{1,0:T(8,128)(2,1)} %get-tuple-element.5) | data formatting | bytes 65536
